TPU v7x, 32 devices: a whole 2x2x4 slice. The times are simulated.
32 devices in a mesh: gr: 2 (over core), fs: 8 (over z, y), tp: 2 (over x).
Axes of the slice: x: 2, y: 2, z: 4, core: 2. Of those that a mesh axis runs over, the one named last changes fastest.
Arguments:
- tokens: bfloat16 [3072, 2048], P(('gr', 'fs')), may hold values from -6 to 6
- routes: int32 [3072, 8], P(('gr', 'fs')), may hold values from 0 to 15, all different within a row; in each aligned block of 192 rows (0 to 191, 192 to 383, ...) at most 144 rows name the same one
- route_weight: float32 [3072, 8], P(('gr', 'fs')), may hold values from 0.05 to 0.6
- norm_gain: float32 [2048], replicated, may hold values from 0.1 to 1.9
- gate_experts: float32 [2, 8, 512, 2048], P('gr', None, 'fs', 'tp'), may hold values from -0.125 to 0.125
- up_experts: float32 [2, 8, 512, 2048], P('gr', None, 'fs', 'tp'), may hold values from -0.125 to 0.125
- down_experts: float32 [2, 8, 512, 2048], P('gr', None, 'fs', 'tp'), may hold values from -0.25 to 0.25
- gate_shared: float32 [2048, 512], P('fs', 'tp'), may hold values from -0.125 to 0.125
- up_shared: float32 [2048, 512], P('fs', 'tp'), may hold values from -0.125 to 0.125
- down_shared: float32 [512, 2048], P('fs', 'tp'), may hold values from -0.25 to 0.25
Outputs:
- mixed: bfloat16 [3072, 2048], P(('gr', 'fs'), 'tp')
- gate_served: bfloat16 [2, 8, 512, 2048], P(None, 'fs', 'tp')
- up_served: bfloat16 [2, 8, 512, 2048], P(None, 'fs', 'tp')
- down_served: bfloat16 [2, 8, 512, 2048], P(None, 'fs', None, 'tp')
- gate_shared_served: bfloat16 [2048, 512], P(None, 'tp')
- up_shared_served: bfloat16 [2048, 512], P(None, 'tp')
- down_shared_served: bfloat16 [512, 2048], P(None, 'tp')
Inputs may be any that keep to these rules, and one draw needn't show every extreme that they name: `routes`: each row names 8 different experts; within the 192 rows of one device no expert is named by more than 144 rows, and some expert reaches 144.
All inputs are finite; a program needn't handle non-finite values.
Results may differ from a plain program's by a relative error of at most 0.0084.
Values may be sent and summed in bfloat16 or wider, within the bound.
A program may use at most 128 MiB of HBM per device.

v0:
```python
import functools

import jax
import jax.numpy as jnp
from jax import lax
from jax.experimental import pallas as pl
from jax.experimental.pallas import tpu as pltpu
from jax.sharding import PartitionSpec as P

EPS = 1e-06
MESH = pl.DeviceIdType.MESH


def greet_group(dims, gr, fs, tp, barrier):
    n_gr, n_fs, n_tp = dims

    def greet(i, carry):
        f, t = i // n_tp, i % n_tp

        @pl.when((f != fs) | (t != tp))
        def _():
            pl.semaphore_signal(barrier, inc=1, device_id=(gr, f, t), device_id_type=MESH)
        return carry

    lax.fori_loop(0, n_fs * n_tp, greet, 0)
    for p in range(1, n_gr):
        pl.semaphore_signal(
            barrier, inc=1, device_id=((gr + p) % n_gr, fs, tp), device_id_type=MESH
        )
    pl.semaphore_wait(barrier, n_fs * n_tp - 1 + n_gr - 1)


def forward(n_gr, block, s_sem, r_sem, p):
    gr, fs, tp = lax.axis_index("gr"), lax.axis_index("fs"), lax.axis_index("tp")
    return pltpu.make_async_remote_copy(
        src_ref=block, dst_ref=block, send_sem=s_sem, recv_sem=r_sem,
        device_id=((gr + p) % n_gr, fs, tp), device_id_type=MESH,
    )


def wide_steps(dims, g_loc, u_loc, g_out, u_out, send, recv, own, f_send, f_recv):
    n_gr, n_fs, n_tp = dims
    gr, fs, tp = lax.axis_index("gr"), lax.axis_index("fs"), lax.axis_index("tp")
    held = g_loc.shape[0] // n_fs
    rows, cols = g_loc.shape[1], g_loc.shape[2]
    per = g_out.shape[2] // rows
    to_tp = fs // per

    def place(out):
        return out.at[gr, :, pl.ds(pl.multiple_of((fs % per) * rows, rows), rows),
                      pl.ds(pl.multiple_of(tp * cols, cols), cols)]

    def wide(loc, out, m, d):
        k = (fs + d) % n_fs
        return pltpu.make_async_remote_copy(
            src_ref=loc.at[pl.ds(k * held, held)], dst_ref=place(out),
            send_sem=send.at[m, d], recv_sem=recv.at[m, fs % per, tp],
            device_id=(gr, k, to_tp), device_id_type=MESH,
        )

    def wide_own(loc, out, m):
        return pltpu.make_async_copy(loc.at[pl.ds(fs * held, held)], place(out), own.at[m])

    def block(out, g, j, t):
        return out.at[g, :, pl.ds(j * rows, rows), pl.ds(t * cols, cols)]

    pairs = ((g_loc, g_out, 0), (u_loc, u_out, 1))
    for loc, out, m in pairs:
        for d in range(1, n_fs):
            wide(loc, out, m, d).start()

        @pl.when(to_tp == tp)
        def _():
            wide_own(loc, out, m).start()

        @pl.when(to_tp != tp)
        def _():
            wide(loc, out, m, 0).start()
        yield
    for loc, out, m in pairs:
        for j in range(per):
            for t in range(n_tp):
                here = (tp * per + j == fs) & (tp == t)
                part = block(out, gr, j, t)

                @pl.when(here)
                def _():
                    wide_own(loc, out, m).wait()

                @pl.when(jnp.logical_not(here))
                def _():
                    forward(n_gr, part, recv.at[m, j, t], recv.at[m, j, t], 1).wait_recv()
                for p in range(1, n_gr):
                    forward(n_gr, part, f_send.at[m, j, t, p - 1], f_recv.at[m, j, t, p - 1], p).start()
        yield
    for loc, out, m in pairs:
        for d in range(1, n_fs):
            wide(loc, out, m, d).wait_send()

        @pl.when(to_tp != tp)
        def _():
            wide(loc, out, m, 0).wait_send()
        for j in range(per):
            for t in range(n_tp):
                for p in range(1, n_gr):
                    sems = f_send.at[m, j, t, p - 1], f_recv.at[m, j, t, p - 1]
                    forward(n_gr, block(out, gr, j, t), *sems, p).wait_send()
                    forward(n_gr, block(out, (gr + n_gr - p) % n_gr, j, t), *sems, p).wait_recv()


def tall_steps(dims, d_loc, d_out, send, recv, own, f_send, f_recv):
    n_gr, n_fs, n_tp = dims
    gr, fs, tp = lax.axis_index("gr"), lax.axis_index("fs"), lax.axis_index("tp")
    held = d_loc.shape[0] // n_fs
    rows = d_loc.shape[1]

    def block(g, s):
        start = s * rows if isinstance(s, int) else pl.multiple_of(s * rows, rows)
        return d_out.at[g, :, pl.ds(start, rows), :]

    def tall(d):
        k = (fs + d) % n_fs
        return pltpu.make_async_remote_copy(
            src_ref=d_loc.at[pl.ds(k * held, held)], dst_ref=block(gr, fs),
            send_sem=send.at[d], recv_sem=recv.at[fs],
            device_id=(gr, k, tp), device_id_type=MESH,
        )

    mine = pltpu.make_async_copy(d_loc.at[pl.ds(fs * held, held)], block(gr, fs), own)
    for d in range(1, n_fs):
        tall(d).start()
    mine.start()
    yield
    for s in range(n_fs):
        @pl.when(s == fs)
        def _():
            mine.wait()

        @pl.when(s != fs)
        def _():
            forward(n_gr, block(gr, s), recv.at[s], recv.at[s], 1).wait_recv()
        for p in range(1, n_gr):
            forward(n_gr, block(gr, s), f_send.at[s, p - 1], f_recv.at[s, p - 1], p).start()
    yield
    for d in range(1, n_fs):
        tall(d).wait_send()
    for s in range(n_fs):
        for p in range(1, n_gr):
            sems = f_send.at[s, p - 1], f_recv.at[s, p - 1]
            forward(n_gr, block(gr, s), *sems, p).wait_send()
            forward(n_gr, block((gr + n_gr - p) % n_gr, s), *sems, p).wait_recv()


def gather_steps(dims, inner, number, *refs):
    n_gr, n_fs, n_tp = dims
    gr, fs, tp = lax.axis_index("gr"), lax.axis_index("fs"), lax.axis_index("tp")
    ins, outs = refs[:number], refs[number:2 * number]
    z_send, z_recv, y_send, y_recv, own = refs[2 * number:]
    nz = n_fs // inner
    z, y = fs // inner, fs % inner

    def when_next(way, act):
        pl.when(z < nz - 1 if way == 0 else z > 0)(act)

    def beside(way):
        return (gr, (z + 1 if way == 0 else z - 1) * inner + y, tp)

    def block(m, zz, yy):
        rows = ins[m].shape[0]
        return outs[m].at[pl.ds(pl.multiple_of((zz * inner + yy) * rows, rows), rows), :]

    def at(way, d):
        return z - d if way == 0 else z + d

    def z_copy(m, way, d):
        return pltpu.make_async_remote_copy(
            src_ref=ins[m] if d == 0 else block(m, at(way, d), y), dst_ref=block(m, at(way, d), y),
            send_sem=z_send.at[m, way, d], recv_sem=z_recv.at[m, way, d],
            device_id=beside(way), device_id_type=MESH,
        )

    def z_landed(m, way, d):
        part = block(m, at(way, d), y)
        pltpu.make_async_remote_copy(
            src_ref=part, dst_ref=part, send_sem=z_send.at[m, way, d - 1],
            recv_sem=z_recv.at[m, way, d - 1], device_id=beside(way), device_id_type=MESH,
        ).wait_recv()

    def y_copy(m, q, way, d, source):
        part = block(m, at(way, d), source)
        i = d + way * (nz - 1) if d else 0
        return pltpu.make_async_remote_copy(
            src_ref=ins[m] if d == 0 else part, dst_ref=part,
            send_sem=y_send.at[m, q - 1, i], recv_sem=y_recv.at[m, q - 1, i],
            device_id=(gr, z * inner + (y + q) % inner, tp), device_id_type=MESH,
        )

    def own_copy(m):
        return pltpu.make_async_copy(ins[m], block(m, z, y), own.at[m])

    def steps(d, way, act):
        if d == 0:
            act()
        else:
            pl.when(z - d >= 0 if way == 0 else z + d < nz)(act)

    places = [(0, 0)] + [(d, way) for d in range(1, nz) for way in (0, 1)]
    for m in range(number):
        for way in (0, 1):
            when_next(way, lambda m=m, way=way: z_copy(m, way, 0).start())
        for q in range(1, inner):
            y_copy(m, q, 0, 0, y).start()
    for m in range(number):
        own_copy(m).start()
    yield
    for d, way in places[1:]:
        def pass_on(d=d, way=way):
            for m in range(number):
                z_landed(m, way, d)
                if d < nz - 1:
                    when_next(way, lambda: z_copy(m, way, d).start())
                for q in range(1, inner):
                    y_copy(m, q, way, d, y).start()
        steps(d, way, pass_on)
        if way:
            yield
    for m in range(number):
        for way in (0, 1):
            when_next(way, lambda m=m, way=way: z_copy(m, way, 0).wait_send())
    for d, way in places:
        def finish(d=d, way=way):
            for m in range(number):
                if 0 < d < nz - 1:
                    when_next(way, lambda: z_copy(m, way, d).wait_send())
                for q in range(1, inner):
                    y_copy(m, q, way, d, y).wait_send()
                    y_copy(m, q, way, d, (y + inner - q) % inner).wait_recv()
        steps(d, way, finish)
    for m in range(number):
        own_copy(m).wait()


def run_steps(first, second):
    live = [first, second]
    while live:
        for steps in list(live):
            if next(steps, live) is live:
                live.remove(steps)


def fused_kernel(dims, inner, number, main_steps, main_ins, main_outs, main_sems, *refs):
    gr, fs, tp = lax.axis_index("gr"), lax.axis_index("fs"), lax.axis_index("tp")
    greet_group(dims, gr, fs, tp, pltpu.get_barrier_semaphore())
    edges = [0]
    for n in (number, main_ins, number, main_outs, 5, main_sems):
        edges.append(edges[-1] + n)
    a, b, c, d, e, f = [refs[edges[i]:edges[i + 1]] for i in range(6)]
    run_steps(gather_steps(dims, inner, number, *a, *c, *e), main_steps(dims, *b, *d, *f))


def exchange(dims, ident, work, main_steps, arrays, main_args, main_outs, main_sems):
    n_fs = dims[1]
    inner = 2 if n_fs % 2 == 0 else 1
    nz = n_fs // inner
    number = len(arrays)
    outs = tuple(jax.ShapeDtypeStruct((n_fs * a.shape[0], a.shape[1]), a.dtype) for a in arrays)
    chain = (number, 2, max(1, nz - 1))
    across = (number, max(1, inner - 1), 2 * nz - 1)
    sems = [chain, chain, across, across, (number,), *main_sems]
    args = (*arrays, *main_args)
    outs = outs + tuple(main_outs)
    return pl.pallas_call(
        functools.partial(
            fused_kernel, dims, inner, number, main_steps,
            len(main_args), len(main_outs), len(main_sems),
        ),
        out_shape=outs,
        in_specs=[pl.BlockSpec(memory_space=pl.ANY)] * len(args),
        out_specs=tuple(pl.BlockSpec(memory_space=pl.ANY) for _ in outs),
        scratch_shapes=[pltpu.SemaphoreType.DMA(shape) for shape in sems],
        compiler_params=pltpu.CompilerParams(collective_id=ident, has_side_effects=True),
        cost_estimate=pl.CostEstimate(flops=0, bytes_accessed=work, transcendentals=0),
    )(*args)


def exchange_wide(dims, rows_here, g_loc, u_loc):
    n_gr, n_fs, n_tp = dims
    count, rows, cols = g_loc.shape
    per = n_fs // n_tp
    out = jax.ShapeDtypeStruct((n_gr, count // n_fs, per * rows, n_tp * cols), g_loc.dtype)
    halves = (2, per, n_tp, n_gr - 1)
    return exchange(
        dims, 1, 200 << 20, wide_steps, (rows_here,), (g_loc, u_loc), (out, out),
        [(2, n_fs), (2, per, n_tp), (2,), halves, halves],
    )


def exchange_tall(dims, shared_here, d_loc):
    n_gr, n_fs, n_tp = dims
    count, rows, cols = d_loc.shape
    out = jax.ShapeDtypeStruct((n_gr, count // n_fs, n_fs * rows, cols), d_loc.dtype)
    return exchange(
        dims, 2, 100 << 20, tall_steps, shared_here, (d_loc,), (out,),
        [(n_fs,), (n_fs,), (), (n_fs, n_gr - 1), (n_fs, n_gr - 1)],
    )


def on_device(tokens, routes, route_weight, norm_gain, gate_experts, up_experts, down_experts,
              gate_shared, up_shared, down_shared):
    bf = jnp.bfloat16
    f32 = jnp.float32
    dims = (lax.axis_size("gr"), lax.axis_size("fs"), lax.axis_size("tp"))
    n_gr, n_fs, n_tp = dims
    fs_index = lax.axis_index("fs")
    tp_index = lax.axis_index("tp")
    cols = gate_experts.shape[3]
    per_group = gate_experts.shape[1]
    count = per_group * n_gr
    held = per_group // n_fs
    tok_count, top = routes.shape
    width = tokens.shape[1]

    values = tokens.astype(f32)
    normed = (values * lax.rsqrt(jnp.mean(values * values, axis=-1, keepdims=True) + EPS)).astype(bf)
    named = routes[:, :, None] == jnp.arange(count, dtype=jnp.int32)[None, None, :]
    weight = jnp.sum(jnp.where(named, route_weight[:, :, None], 0.0), axis=1)
    high = lax.reduce_precision(weight, 8, 7)
    extra = -(-2 * count // 128) * 128
    tail = jnp.concatenate(
        [high.astype(bf), (weight - high).astype(bf), jnp.zeros((tok_count, extra - 2 * count), bf)],
        axis=1,
    )
    rows_here = jnp.concatenate([normed, tail], axis=1)

    gain_shared = lax.dynamic_slice_in_dim(
        norm_gain, fs_index * gate_shared.shape[0], gate_shared.shape[0], 0
    )
    shared_here = (
        (gate_shared * gain_shared[:, None]).astype(bf),
        (up_shared * gain_shared[:, None]).astype(bf),
        down_shared.astype(bf),
    )

    gain_cols = lax.dynamic_slice_in_dim(norm_gain, tp_index * cols, cols, 0)
    rows_all, gate_w, up_w = exchange_wide(
        dims,
        rows_here,
        (gate_experts[0] * gain_cols[None, None, :]).astype(bf),
        (up_experts[0] * gain_cols[None, None, :]).astype(bf),
    )

    x = rows_all[:, :width]
    w_all = (
        rows_all[:, width:width + count].astype(f32)
        + rows_all[:, width + count:width + 2 * count].astype(f32)
    )
    units = gate_w.shape[2]
    parts = []
    for g in range(n_gr):
        w_here = lax.dynamic_slice_in_dim(w_all, g * per_group + fs_index * held, held, 1)
        for k in range(held):
            gate = lax.dot_general(x, gate_w[g, k], (((1,), (1,)), ((), ())), preferred_element_type=f32)
            upper = lax.dot_general(x, up_w[g, k], (((1,), (1,)), ((), ())), preferred_element_type=f32)
            parts.append((jax.nn.silu(gate) * upper * w_here[:, k:k + 1]).astype(bf))
    hidden = jnp.stack(parts)
    hidden, down_local, shared_here = lax.optimization_barrier(
        (hidden, down_experts[0].astype(bf), shared_here)
    )
    gate_sw, up_sw, down_sw, down_w = exchange_tall(dims, shared_here, down_local)
    hidden = lax.all_gather(hidden, "tp", axis=0, tiled=False)
    partial = jnp.zeros((), f32)
    down_flat = down_w.reshape(n_gr * held, n_tp, units, cols)
    for i in range(n_gr * held):
        for t in range(n_tp):
            partial = partial + jnp.dot(hidden[t, i], down_flat[i, t], preferred_element_type=f32)
    partial, normed = lax.optimization_barrier((partial.astype(bf), normed))
    routed = lax.psum_scatter(partial, "fs", scatter_dimension=0, tiled=True)

    shared_hidden = (
        jax.nn.silu(jnp.dot(normed, gate_sw, preferred_element_type=f32))
        * jnp.dot(normed, up_sw, preferred_element_type=f32)
    ).astype(bf)
    shared_full = lax.all_gather(shared_hidden, "tp", axis=1, tiled=True)
    shared = jnp.dot(shared_full, down_sw, preferred_element_type=f32)
    mixed = (routed.astype(f32) + shared).astype(bf)
    return (mixed, gate_w, up_w, down_w, gate_sw, up_sw, down_sw)


def solution(mesh):
    return jax.shard_map(
        on_device,
        mesh=mesh,
        in_specs=(
            P(("gr", "fs"), None),
            P(("gr", "fs"), None),
            P(("gr", "fs"), None),
            P(),
            P("gr", None, "fs", "tp"),
            P("gr", None, "fs", "tp"),
            P("gr", None, "fs", "tp"),
            P("fs", "tp"),
            P("fs", "tp"),
            P("fs", "tp"),
        ),
        out_specs=(
            P(("gr", "fs"), "tp"),
            P(None, "fs", "tp", None),
            P(None, "fs", "tp", None),
            P(None, "fs", None, "tp"),
            P(None, "tp"),
            P(None, "tp"),
            P(None, "tp"),
        ),
        check_vma=False,
    )
```

profile of v0, /device:TPU:0, one launch (start us, length us, event | category | flops | bytes accessed | tf_op | source)
XLA Modules:
  0.0 315.8 jit_solution(10333539815235602071)
XLA Ops:
  7.2 0.9 select_reduce_fusion
  8.4 1.4 fusion.34
  9.8 1.3 fusion.35
  11.2 3.5 %fusion.32 = (bf16[8,64,1024]{2,1,0:T(8,128)(2,1)}, bf16[8,64,1024]{2,1,0:T(8,128)(2,1)}) fusion(f32[1,8,64,1024]{3,2,1,0:T(8,128)S(1)} %copy-done.7, f32[1024]{0:T(1024)S(1)} %dynamic_slice.12, f32[1,8,64,1024]{3,2,1,0:T(8,128)} %param.14), kind=kLoop, calls=%fused_computation.18 | loop fusion | flops 2097152 | bytes 6295552 | tf_op jit(solution)/shard_map/convert_element_type | solution.py:349
  14.7 1.1 concatenate.3.refs_0_
  15.8 122.3 %shard_map.153 = (bf16[1536,2176]{1,0:T(8,128)(2,1)}, bf16[2,1,256,2048]{3,2,1,0:T(8,128)(2,1)}, bf16[2,1,256,2048]{3,2,1,0:T(8,128)(2,1)}) custom-call(bf16[192,2176]{1,0:T(8,128)(2,1)} %concatenate.3.refs_0_, bf16[8,64,1024]{2,1,0:T(8,128)(2,1)} %get-tuple-element.40.refs_1_, bf16[8,64,1024]{2,1,0:T(8,128)(2,1)} %get-tuple-element.39.refs_2_), custom_call_target="tpu_custom_call" | custom-call | bytes 209715200 | tf_op jit(solution)/shard_map/pallas_call | solution.py:272
  138.1 1.4 convert_add_fusion
  139.5 6.2 %fusion.6 = f32[1536,256]{1,0:T(8,128)} fusion(bf16[1536,2176]{1,0:T(8,128)(2,1)} %get-tuple-element.21, bf16[2,1,256,2048]{3,2,1,0:T(8,128)(2,1)} %get-tuple-element.51), kind=kOutput, calls=%fused_computation.7 | convolution fusion | flops 1610612736 | bytes 8912896 | tf_op jit(solution)/shard_map/dot_general | solution.py:362
  145.7 3.0 fusion.2
  148.8 2.8 convert_bitcast_fusion.refs_3_
  151.6 0.7 convert_element_type.71.refs_2_
  152.3 0.9 dynamic-slice_reduce_fusion.1
  153.3 5.5 %fusion.26 = bf16[1,1536,256]{2,1,0:T(8,128)(2,1)S(1)} fusion(bf16[1536,2176]{1,0:T(8,128)(2,1)} %get-tuple-element.21, f32[1536,256]{1,0:T(8,128)S(1)} %copy-done.14, bf16[2,1,256,2048]{3,2,1,0:T(8,128)(2,1)} %get-tuple-element.52, f32[1536]{0:T(1024)S(1)} %get-tuple-element.35), kind=kOutput, calls=%fused_computation.15 | convolution fusion | flops 1613365248 | bytes 9705472 | tf_op jit(solution)/shard_map/dot_general | solution.py:363
  158.8 2.1 fusion.29
  160.9 1.3 pad_maximum_fusion
  162.2 0.8 multiply_convert_fusion
  163.1 53.6 %shard_map.154 = (bf16[2048,256]{1,0:T(8,128)(2,1)}, bf16[2048,256]{1,0:T(8,128)(2,1)}, bf16[512,1024]{1,0:T(8,128)(2,1)}, bf16[2,1,512,1024]{3,2,1,0:T(8,128)(2,1)}) custom-call(bf16[256,256]{1,0:T(8,128)(2,1)} %get-tuple-element.25.refs_0_, bf16[256,256]{1,0:T(8,128)(2,1)} %get-tuple-element.26.refs_1_, bf16[64,1024]{1,0:T(8,128)(2,1)} %convert_element_type.71.refs_2_, ...), custom_call_target="tpu_custom_call" | custom-call | bytes 104857600 | tf_op jit(solution)/shard_map/pallas_call | solution.py:272
  216.8 2.4 fusion.47
  219.7 1.0 fusion.48
  220.6 1.0 fusion.46
  221.6 2.8 add_convert_fusion
  224.4 1.6 fusion.50
  226.0 1.6 fusion.37
  227.6 5.3 %all_gather.11 = bf16[192,512]{1,0:T(8,128)(2,1)S(1)} all-gather(bf16[192,256]{1,0:T(8,128)(2,1)S(1)} %fusion.37), channel_id=1, replica_groups=mesh['gr'=2,'fs'=8,'tp'=2] {'tp'}, dimensions={1}, use_global_device_ids=true | all-gather | bytes 294912 | tf_op jit(solution)/shard_map/all_gather | solution.py:383
  232.9 63.4 %reduce-scatter.2.cloned.1.call-done = bf16[192,1024]{1,0:T(8,128)(2,1)} async-done(((bf16[1536,1024]{1,0:T(8,128)(2,1)}), bf16[192,1024]{1,0:T(8,128)(2,1)}) %reduce-scatter.2.cloned.1.call-update) | async-done | bytes 393232 | tf_op jit(solution)/shard_map/reduce_scatter | solution.py:377
  296.4 2.4 fusion.36
  298.8 3.3 %copy.34 = bf16[2,1,256,2048]{3,2,1,0:T(8,128)(2,1)} copy(bf16[2,1,256,2048]{3,2,1,0:T(8,128)(2,1)} %get-tuple-element.51) | data formatting | bytes 4194304
  302.1 1.3 copy.35
  303.5 1.3 copy.36
  305.4 1.0 copy.37
  307.0 1.0 copy.38
  308.0 1.0 copy.39
  (54 shorter events, 2.4 us)
Async XLA Ops:
  7.2 4.0 %copy-start.12 = (f32[2048]{0:T(1024)S(1)}, f32[2048]{0:T(1024)}, u32[]{:S(2)}) copy-start(f32[2048]{0:T(1024)} %param.13) | copy-start | bytes 24580
  7.2 4.0 %copy-start.7 = (f32[1,8,64,1024]{3,2,1,0:T(8,128)S(1)}, f32[1,8,64,1024]{3,2,1,0:T(8,128)}, u32[]{:S(2)}) copy-start(f32[1,8,64,1024]{3,2,1,0:T(8,128)} %param.15) | copy-start | bytes 6291460
  7.2 209.5 %all-gather.3.cloned.1.call-start = ((), (), s32[]{:S(2)}) async-start(), calls=%async_computation.2 | async-start | bytes 4718592 | tf_op jit(solution)/shard_map/all_gather | solution.py:370
  138.1 7.7 %slice-start = ((s8[6684672]{0:T(1024)(128)(4,1)}), s8[4194304]{0:T(1024)(128)(4,1)S(1)}, s32[]{:S(2)}) async-start(s8[6684672]{0:T(1024)(128)(4,1)} %bitcast.66), calls=%async_computation.3 | async-start | bytes 8388608
  139.5 6.2 %copy-start.6 = (bf16[2,1,256,2048]{3,2,1,0:T(8,128)(2,1)S(1)}, bf16[2,1,256,2048]{3,2,1,0:T(8,128)(2,1)}, u32[]{:S(2)}) copy-start(bf16[2,1,256,2048]{3,2,1,0:T(8,128)(2,1)} %get-tuple-element.51) | copy-start | bytes 6291460
  139.5 6.2 %slice-start.1 = ((s8[6684672]{0:T(1024)(128)(4,1)}), s8[2490368]{0:T(1024)(128)(4,1)S(1)}, s32[]{:S(2)}) async-start(s8[6684672]{0:T(1024)(128)(4,1)} %bitcast.66), calls=%async_computation.4 | async-start | bytes 4980736
  148.7 2.9 copy-start.9
  148.8 4.4 %copy-start.14 = (f32[1536,256]{1,0:T(8,128)S(1)}, f32[1536,256]{1,0:T(8,128)}, u32[]{:S(2)}) copy-start(f32[1536,256]{1,0:T(8,128)} %fusion.6) | copy-start | bytes 4718596
  152.3 6.5 %slice-start.2 = ((s8[6684672]{0:T(1024)(128)(4,1)}), s8[4194304]{0:T(1024)(128)(4,1)S(1)}, s32[]{:S(2)}) async-start(s8[6684672]{0:T(1024)(128)(4,1)} %bitcast.68), calls=%async_computation.5 | async-start | bytes 8388608
  153.2 5.6 %copy-start.4 = (bf16[2,1,256,2048]{3,2,1,0:T(8,128)(2,1)S(1)}, bf16[2,1,256,2048]{3,2,1,0:T(8,128)(2,1)}, u32[]{:S(2)}) copy-start(bf16[2,1,256,2048]{3,2,1,0:T(8,128)(2,1)} %get-tuple-element.52) | copy-start | bytes 6291460
  153.2 5.6 %slice-start.3 = ((s8[6684672]{0:T(1024)(128)(4,1)}), s8[2490368]{0:T(1024)(128)(4,1)S(1)}, s32[]{:S(2)}) async-start(s8[6684672]{0:T(1024)(128)(4,1)} %bitcast.68), calls=%async_computation.6 | async-start | bytes 4980736
  153.2 5.6 %copy-start.13 = (f32[1536,256]{1,0:T(8,128)S(1)}, f32[1536,256]{1,0:T(8,128)}, u32[]{:S(2)}) copy-start(f32[1536,256]{1,0:T(8,128)} %fusion.2) | copy-start | bytes 4718596
  160.9 1.3 copy-start.10
  160.9 1.3 copy-start.11
  163.1 133.3 %reduce-scatter.2.cloned.1.call-start = ((), (), s32[]{:S(2)}) async-start(), calls=%async_computation.1 | async-start | bytes 3538944 | tf_op jit(solution)/shard_map/reduce_scatter | solution.py:377
  216.7 2.4 copy-start
  216.8 2.9 copy-start.1
  298.8 3.3 %copy-start.5 = (bf16[2,1,256,2048]{3,2,1,0:T(8,128)(2,1)S(1)}, bf16[2,1,256,2048]{3,2,1,0:T(8,128)(2,1)}, u32[]{:S(2)}) copy-start(bf16[2,1,256,2048]{3,2,1,0:T(8,128)(2,1)} %get-tuple-element.52) | copy-start | bytes 6291460
  303.5 2.0 copy-start.3
  305.4 1.6 copy-start.8
  305.4 2.6 copy-start.2
Sparse Core Ops, SparseCore 0:
  163.2 42.0 all-gather.2
  224.6 71.7 reduce-scatter.1
where the time goes:
time: 316 us
  Pallas kernels  176 us (56%)
  waiting for transfers between devices  63.5 us (20%)
  matrix products  29.6 us (9%)
  between operations  14.3 us (5%)
  other arithmetic  14.1 us (4%)
  local copies, waits for them, and re-layouts  13.1 us (4%)
  blocking collectives  5.29 us (2%)
    pallas_call x2, Pallas kernels, exchange(): pl.pallas_call(functools.partial(fused_kernel, dims, inner, number, main_...  176 us
    reduce_scatter x1, waiting for transfers between devices, on_device(): routed = lax.psum_scatter(partial, 'fs', scatter_dimension=0, tiled=True)  63.4 us
    unnamed x44, local copies, waits for them, and re-layouts  10.7 us
    dot_general x2, matrix products, on_device(): lax.dot_general(x, gate_w[g, k], (((1,), (1,)), ((), ())), preferred_elem...  9.16 us
    dot_general x2, matrix products, on_device(): lax.dot_general(x, up_w[g, k], (((1,), (1,)), ((), ())), preferred_elemen...  7.6 us
    dot_general x4, matrix products, on_device(): jnp.dot(hidden[t, i], down_flat[i, t], preferred_element_type=f32)  7.16 us
  transfers between devices with their start and end apart: 2, of which 1 were waited for; matrix products, arithmetic and copies ran while one was open for 1% of the time, Pallas kernels for 17%

commit v1 on v0

v1 whole, which is shorter than its diff:
```python
import functools

import jax
import jax.numpy as jnp
from jax import lax
from jax.experimental import pallas as pl
from jax.experimental.pallas import tpu as pltpu
from jax.sharding import PartitionSpec as P

EPS = 1e-06
MESH = pl.DeviceIdType.MESH
BF = jnp.bfloat16
F32 = jnp.float32


def whole(cfg, rows_in, local_in, gate_l, up_l, down_l, gs_l, us_l, ds_l,
          mixed_o, gate_o, up_o, down_o, gs_o, us_o, ds_o,
          X, W, H, GS, US, DS, SH, SO, PS, YR, S, ZS, ZR, FS, FR,
          b_send, b_recv, b_own, x_send, x_recv, p_send, p_recv,
          c_zs, c_zr, c_ys, c_yr, c_own, g_send, g_recv,
          sh_send, sh_recv, y_send, y_recv, z_send, z_recv, f_send, f_recv, o_sem):
    n_gr, n_fs, n_tp = cfg.dims
    inner, nz, R, NT, CT = cfg.inner, cfg.nz, cfg.R, cfg.NT, cfg.CT
    gr, fs, tp = lax.axis_index("gr"), lax.axis_index("fs"), lax.axis_index("tp")
    z, y = fs // inner, fs % inner
    rows, cols = gate_l.shape[1], gate_l.shape[2]
    width = cols * n_tp
    depth = rows * n_fs
    units = depth // n_tp
    locs = (gate_l, up_l, down_l)

    def ds(start, size):
        if isinstance(start, int):
            return pl.ds(start, size)
        return pl.ds(pl.multiple_of(start * 1, size), size)

    def remote(src, dst, s, r, to):
        return pltpu.make_async_remote_copy(
            src_ref=src, dst_ref=dst, send_sem=s, recv_sem=r, device_id=to, device_id_type=MESH)

    barrier = pltpu.get_barrier_semaphore()

    def greet(d, c):
        pl.semaphore_signal(barrier, inc=1, device_id=(gr, (fs + d) % n_fs, tp), device_id_type=MESH)
        return c
    lax.fori_loop(1, n_fs, greet, 0)
    for q in range(1, n_tp):
        pl.semaphore_signal(barrier, inc=1, device_id=(gr, fs, (tp + q) % n_tp), device_id_type=MESH)
    for p in range(1, n_gr):
        pl.semaphore_signal(barrier, inc=1, device_id=((gr + p) % n_gr, fs, tp), device_id_type=MESH)
    pl.semaphore_wait(barrier, n_fs - 1 + n_tp - 1 + n_gr - 1)

    def block(m, s, t):
        return W.at[m, gr, ds(s * rows, rows), ds(t * cols, cols)]

    def region(m, g, t):
        return W.at[m, g, :, ds(t * cols, cols)]

    def to_expert(m, k):
        return remote(locs[m].at[k], block(m, fs, tp), b_send.at[m], b_recv.at[m, fs], (gr, k, tp))

    def own_block(m):
        return pltpu.make_async_copy(locs[m].at[fs], block(m, fs, tp), b_own.at[m])

    def each_other(act):
        def step(d, c):
            pl.when(fs + d < n_fs)(lambda: act(fs + d))
            pl.when(fs - d >= 0)(lambda: act(fs - d))
            return c
        lax.fori_loop(1, n_fs, step, 0)

    def across(m, src, s):
        for q in range(1, n_tp):
            remote(src, block(m, s, tp), x_send.at[m, q - 1], x_recv.at[m, q - 1],
                   (gr, fs, (tp + q) % n_tp)).start()

    def send_matrix(m):
        each_other(lambda k: to_expert(m, k).start())
        own_block(m).start()
        across(m, locs[m].at[fs], fs)

    def landed(m, s):
        part = block(m, s, tp)
        remote(part, part, b_recv.at[m, s], b_recv.at[m, s], (gr, s, tp)).wait_recv()
        across(m, part, s)

    def partner(m, g, q, p):
        part = region(m, g, (tp + n_tp - q) % n_tp)
        return remote(part, part, p_send.at[m, q, p - 1], p_recv.at[m, q, p - 1],
                      ((gr + p) % n_gr, fs, tp))

    def share(m, q):
        for p in range(1, n_gr):
            partner(m, gr, q, p).start()

    def shared_landed(m, q):
        for p in range(1, n_gr):
            partner(m, (gr + n_gr - p) % n_gr, q, p).wait_recv()

    def x_landed(m, q):
        part = region(m, gr, (tp + n_tp - q) % n_tp)
        remote(part, part, x_send.at[m, q - 1], x_recv.at[m, q - 1],
               (gr, fs, (tp + q) % n_tp)).wait_recv()

    big = ((rows_in, lambda zz, yr: X.at[ds((yr * nz + zz) * R, R), :], 1),)

    def shared_item(src, dst, parts):
        size = src.shape[0] // parts

        def place(zz, yr):
            f = zz * inner + (y + yr) % inner
            if parts == 1:
                return dst.at[ds(f * size, size), :]
            return dst.at[ds((f * parts + gr) * size, size), :]
        own = src if parts == 1 else src.at[ds(gr * size, size), :]
        return (own, place, parts)
    small = tuple(shared_item(s, d, p) for s, d, p in zip((gs_l, us_l, ds_l), (GS, US, DS), cfg.parts))
    items = big + small

    def at(way, d):
        return z - d if way == 0 else z + d

    def z_copy(m, way, d):
        own, place, _ = items[m]
        dst = place(at(way, d), 0)
        return remote(own if d == 0 else dst, dst, c_zs.at[m, way, d], c_zr.at[m, way, d],
                      (gr, (z + 1 if way == 0 else z - 1) * inner + y, tp))

    def y_slot(d, way):
        return d + way * (nz - 1) if d else 0

    def y_copy(m, q, way, d):
        own, place, parts = items[m]
        zz = at(way, d)
        src = own if d == 0 else place(zz, 0)
        dst = place(zz, inner - q) if m == 0 else place(zz, 0)
        i = y_slot(d, way)
        return remote(src, dst, c_ys.at[m, q - 1, i], c_yr.at[m, q - 1, i],
                      (gr, z * inner + (y + q) % inner, tp))

    def pass_partner(m, part):
        if items[m][2] > 1:
            for p in range(1, n_gr):
                remote(part, part, g_send.at[m, p - 1], g_recv.at[m, p - 1],
                       ((gr + p) % n_gr, fs, tp)).start()

    def next_there(way):
        return (z < nz - 1) if way == 0 else (z > 0)

    def there(d, way):
        return (z - d >= 0) if way == 0 else (z + d < nz)

    def gather_start(m):
        own, place, parts = items[m]
        for way in (0, 1):
            pl.when(next_there(way))(lambda way=way: z_copy(m, way, 0).start())
        for q in range(1, inner):
            y_copy(m, q, 0, 0).start()
        pltpu.make_async_copy(own, place(z, 0), c_own.at[m]).start()

    def gather_own(m):
        own, place, parts = items[m]
        pltpu.make_async_copy(own, place(z, 0), c_own.at[m]).wait()
        pass_partner(m, place(z, 0))

    def gather_pass(m, d):
        for way in (0, 1):
            def act(way=way):
                part = items[m][1](at(way, d), 0)
                remote(part, part, c_zs.at[m, way, d - 1], c_zr.at[m, way, d - 1],
                       (gr, (z + 1 if way == 0 else z - 1) * inner + y, tp)).wait_recv()
                if d < nz - 1:
                    pl.when(next_there(way))(lambda: z_copy(m, way, d).start())
                for q in range(1, inner):
                    y_copy(m, q, way, d).start()
                pass_partner(m, part)
            pl.when(there(d, way))(act)

    places = [(0, 0)] + [(d, way) for d in range(1, nz) for way in (0, 1)]

    def gather_y(m):
        for d, way in places:
            def act(d=d, way=way):
                for q in range(1, inner):
                    part = items[m][1](at(way, d), inner - q)
                    i = y_slot(d, way)
                    remote(part, part, c_ys.at[m, q - 1, i], c_yr.at[m, q - 1, i],
                           (gr, z * inner + (y + q) % inner, tp)).wait_recv()
                    pass_partner(m, part)
            if d == 0:
                act()
            else:
                pl.when(there(d, way))(act)

    def gather_sent(m):
        for d, way in places:
            def act(d=d, way=way):
                for w in ((0, 1) if d == 0 else (way,)):
                    if d < nz - 1:
                        pl.when(next_there(w))(lambda w=w: z_copy(m, w, d).wait_send())
                for q in range(1, inner):
                    y_copy(m, q, way, d).wait_send()
            if d == 0:
                act()
            else:
                pl.when(there(d, way))(act)

    def partner_gathered(m, way):
        dst = (X, GS, US, DS)[m]
        if items[m][2] > 1:
            part = dst.at[pl.ds(0, dst.shape[0] // items[m][2]), :]
            for p in range(1, n_gr):
                c = remote(part, part, g_send.at[m, p - 1], g_recv.at[m, p - 1],
                           ((gr + p) % n_gr, fs, tp))
                if way:
                    c.wait_send()
                else:
                    c.wait_recv()

    gather_start(0)
    send_matrix(0)
    if nz > 1:
        gather_pass(0, 1)
    send_matrix(1)
    if nz > 2:
        gather_pass(0, 2)
    for m in (1, 2, 3):
        gather_start(m)
    send_matrix(2)
    for d in range(3, nz):
        gather_pass(0, d)
    for m in (1, 2, 3):
        gather_own(m)
    for m in (0, 1):
        each_other(lambda s: landed(m, s))
        own_block(m).wait()
        share(m, 0)
        if m:
            for q in range(1, n_tp):
                x_landed(0, q)
                share(0, q)
    for q in range(1, n_tp):
        x_landed(1, q)
        share(1, q)
    pltpu.make_async_copy(rows_in, items[0][1](z, 0), c_own.at[0]).wait()
    gather_y(0)

    outs = (gate_o, up_o)

    def out_wide(m, g):
        return pltpu.make_async_copy(W.at[m, g, ds(tp * units, units), :], outs[m].at[g, 0], o_sem.at[m, g])

    def out_tall(g):
        return pltpu.make_async_copy(region(2, g, tp), down_o.at[g, 0], o_sem.at[2, g])

    NB = cfg.NB
    per = depth // NB
    chunks = n_gr * per
    count = n_gr * n_fs
    lanes = lax.broadcasted_iota(jnp.int32, (n_fs * R, 128), 1)

    def chunk(i, c):
        gg = (gr + i // per) % n_gr
        n = i % per

        @pl.when(i % per == 0)
        def _():
            @pl.when(i > 0)
            def _():
                for m in (0, 1):
                    for q in range(n_tp):
                        for p in range(1, n_gr):
                            pl.when(i // per == n_gr - p)(
                                lambda m=m, q=q, p=p: partner(m, (gr + n_gr - p) % n_gr, q, p).wait_recv())
            for m in (0, 1):
                out_wide(m, gg).start()
        x = X[:, pl.ds(0, width)]
        expert = gg * n_fs + fs
        weight = jnp.zeros((n_fs * R, 1), F32)
        for k in range(cfg.extra // 128):
            tail = X[:, pl.ds(width + k * 128, 128)].astype(F32)
            pick = (lanes + k * 128 == expert) | (lanes + k * 128 == count + expert)
            weight = weight + jnp.sum(jnp.where(pick, tail, 0.0), axis=1, keepdims=True)
        dn = (((1,), (1,)), ((), ()))
        gate = lax.dot_general(x, W[0, gg, ds(n * NB, NB), :], dn, preferred_element_type=F32)
        upper = lax.dot_general(x, W[1, gg, ds(n * NB, NB), :], dn, preferred_element_type=F32)
        H[:, ds((gg * per + n) * NB, NB)] = (gate / (1.0 + jnp.exp(-gate)) * upper * weight).astype(BF)
        each = -(-(n_fs - 1) // chunks)

        def some(e, c):
            d = 1 + i * each + e

            @pl.when(d < n_fs)
            def _():
                pl.when(fs + d < n_fs)(lambda: landed(2, fs + d))
                pl.when(fs - d >= 0)(lambda: landed(2, fs - d))
            return c
        lax.fori_loop(0, each, some, 0)
        return c
    lax.fori_loop(0, chunks, chunk, 0)
    own_block(2).wait()
    share(2, 0)

    for d in range(1, nz):
        for m in (1, 2, 3):
            gather_pass(m, d)
    for m in (1, 2, 3):
        gather_y(m)
        partner_gathered(m, 0)
    sg = jnp.dot(local_in[...], GS[...], preferred_element_type=F32)
    su = jnp.dot(local_in[...], US[...], preferred_element_type=F32)
    SH[pl.ds(tp, 1)] = (sg / (1.0 + jnp.exp(-sg)) * su).astype(BF)[None]
    shared_outs = [pltpu.make_async_copy(a, b, o_sem.at[3 + i, 0])
                   for i, (a, b) in enumerate(((GS, gs_o), (US, us_o), (DS, ds_o)))]
    for c in shared_outs:
        c.start()
    for q in range(1, n_tp):
        x_landed(2, q)
        share(2, q)

    def sh_copy(q):
        return remote(SH.at[tp], SH.at[tp], sh_send.at[q - 1], sh_recv.at[q - 1],
                      (gr, fs, (tp + q) % n_tp))
    for q in range(1, n_tp):
        sh_copy(q).start()
    shared_landed(2, 0)

    tiles = NT // n_tp
    half = nz * R

    def col(i):
        return (tp * tiles + i) % NT

    def y_out(i, r):
        return remote(PS.at[i, r - 1], YR.at[i, r - 1], y_send.at[i, r - 1], y_recv.at[i, r - 1],
                      (gr, z * inner + (y + r) % inner, tp))

    def produce(i, c):
        @pl.when(i == tiles)
        def _():
            for q in range(1, n_tp):
                shared_landed(2, q)
        part = jnp.zeros((n_fs * R, CT), F32)
        for g in range(n_gr):
            part = part + jnp.dot(H[:, pl.ds(g * depth, depth)], W[2, g, :, ds(col(i) * CT, CT)],
                                  preferred_element_type=F32)
        S[pl.ds(i, 1)] = part[:half][None]
        for r in range(1, inner):
            PS[i, r - 1] = part[r * half:(r + 1) * half].astype(BF)

        @pl.when(i > 0)
        def _():
            for r in range(1, inner):
                y_out(i - 1, r).start()
        return c
    lax.fori_loop(0, NT, produce, 0)
    for r in range(1, inner):
        y_out(NT - 1, r).start()
    for g in range(n_gr):
        out_tall(g).start()

    for q in range(1, n_tp):
        part = SH.at[(tp + n_tp - q) % n_tp]
        remote(part, part, sh_send.at[q - 1], sh_recv.at[q - 1], (gr, fs, (tp + q) % n_tp)).wait_recv()
    total = jnp.zeros((n_tp * R, cols), F32)
    su_n = GS.shape[1]
    for t in range(n_tp):
        total = total + jnp.dot(SH[t], DS[pl.ds(t * su_n, su_n), :], preferred_element_type=F32)
    SO[...] = total

    def z_move(way, i, lo, size, to):
        return remote(ZS.at[way, i, pl.ds(lo, size), :], ZR.at[way, i, pl.ds(lo, size), :],
                      z_send.at[way, i], z_recv.at[way, i], (gr, to * inner + y, tp))

    def upward(i, h):
        lo, size = (h + 1) * R, (nz - 1 - h) * R
        if h > 0:
            z_move(0, i, h * R, (nz - h) * R, z + 1).wait_recv()
            S[i, pl.ds(h * R, R), :] = S[i, pl.ds(h * R, R), :] + ZR[0, i, pl.ds(h * R, R), :].astype(F32)
            ZS[0, i, pl.ds(lo, size), :] = (
                S[i, pl.ds(lo, size), :] + ZR[0, i, pl.ds(lo, size), :].astype(F32)).astype(BF)
        else:
            ZS[0, i, pl.ds(lo, size), :] = S[i, pl.ds(lo, size), :].astype(BF)
        z_move(0, i, lo, size, z + 1).start()

    def downward(i, h):
        zz = nz - 1 - h
        size = zz * R
        if h > 0:
            z_move(1, i, 0, size + R, z - 1).wait_recv()
            S[i, pl.ds(size, R), :] = S[i, pl.ds(size, R), :] + ZR[1, i, pl.ds(size, R), :].astype(F32)
            ZS[1, i, pl.ds(0, size), :] = (
                S[i, pl.ds(0, size), :] + ZR[1, i, pl.ds(0, size), :].astype(F32)).astype(BF)
        else:
            ZS[1, i, pl.ds(0, size), :] = S[i, pl.ds(0, size), :].astype(BF)
        z_move(1, i, 0, size, z - 1).start()

    def f_copy(i, to):
        return remote(FS.at[i], FR.at[tp, i % tiles], f_send.at[i], f_recv.at[tp, i % tiles], (gr, fs, to))

    def finish(i):
        if nz > 1:
            last = (nz - 1) * R

            @pl.when(z == nz - 1)
            def _():
                z_move(0, i, last, R, z - 1).wait_recv()
                S[i, pl.ds(last, R), :] = S[i, pl.ds(last, R), :] + ZR[0, i, pl.ds(last, R), :].astype(F32)

            @pl.when(z == 0)
            def _():
                z_move(1, i, 0, R, z + 1).wait_recv()
                S[i, pl.ds(0, R), :] = S[i, pl.ds(0, R), :] + ZR[1, i, pl.ds(0, R), :].astype(F32)
        mine = S[i, ds(z * R, R), :]

        @pl.when(i < tiles)
        def _():
            at_cols = ds(i * CT, CT)
            mixed_o[tp, :, at_cols] = (mine + SO[ds(tp * R, R), at_cols]).astype(BF)

        @pl.when(i >= tiles)
        def _():
            FS[i] = mine.astype(BF)
            f_copy(i, col(i) // tiles).start()

    def advance(j, c):
        @pl.when(j < NT)
        def _():
            for r in range(1, inner):
                part = YR.at[j, r - 1]
                remote(part, part, y_send.at[j, r - 1], y_recv.at[j, r - 1],
                       (gr, z * inner + (y + r) % inner, tp)).wait_recv()
            S[j] = S[j] + sum([YR[j, r - 1].astype(F32) for r in range(1, inner)], 0.0)
        for h in range(nz - 1):
            i = j - h

            @pl.when((i >= 0) & (i < NT))
            def _(i=i, h=h):
                pl.when(z == h)(lambda: upward(i, h))
                pl.when(z == nz - 1 - h)(lambda: downward(i, h))
        i = j - (nz - 1)
        pl.when(i >= 0)(lambda: finish(i))
        return c
    lax.fori_loop(0, NT + nz - 1, advance, 0)

    def arrive(i, c):
        for q in range(1, n_tp):
            t = (tp + n_tp - q) % n_tp
            part = FR.at[t, i]
            remote(part, part, f_send.at[0], f_recv.at[t, i], (gr, fs, t)).wait_recv()
            at_cols = ds(i * CT, CT)
            mixed_o[t, :, at_cols] = (FR[t, i].astype(F32) + SO[ds(t * R, R), at_cols]).astype(BF)
        return c
    lax.fori_loop(0, tiles, arrive, 0)

    for m in range(3):
        part = locs[m].at[pl.ds(0, n_fs - 1)]
        remote(part, part, b_send.at[m], b_send.at[m], (gr, fs, (tp + 1) % n_tp)).wait_send()
        for q in range(1, n_tp):
            part = region(m, gr, tp)
            remote(part, part, x_send.at[m, q - 1], x_recv.at[m, q - 1],
                   (gr, fs, (tp + q) % n_tp)).wait_send()
        for q in range(n_tp):
            for p in range(1, n_gr):
                partner(m, gr, q, p).wait_send()
    for m in range(4):
        gather_sent(m)
        partner_gathered(m, 1)
    for q in range(1, n_tp):
        sh_copy(q).wait_send()

    def drain(i, c):
        for r in range(1, inner):
            y_out(i, r).wait_send()
        for h in range(nz - 1):
            pl.when(z == h)(lambda h=h: z_move(0, i, (h + 1) * R, (nz - 1 - h) * R, z + 1).wait_send())
            pl.when(z == nz - 1 - h)(lambda h=h: z_move(1, i, 0, (nz - 1 - h) * R, z - 1).wait_send())
        pl.when(i >= tiles)(lambda: f_copy(i, col(i) // tiles).wait_send())
        return c
    lax.fori_loop(0, NT, drain, 0)
    for g in range(n_gr):
        out_tall(g).wait()
        for m in (0, 1):
            out_wide(m, g).wait()
    for c in shared_outs:
        c.wait()


class Config:
    pass


def on_device(tokens, routes, route_weight, norm_gain, gate_experts, up_experts, down_experts,
              gate_shared, up_shared, down_shared):
    dims = (lax.axis_size("gr"), lax.axis_size("fs"), lax.axis_size("tp"))
    n_gr, n_fs, n_tp = dims
    fs_index = lax.axis_index("fs")
    tp_index = lax.axis_index("tp")
    per_group, rows, cols = gate_experts.shape[1:]
    count = per_group * n_gr
    assert per_group == n_fs
    tok_count, top = routes.shape
    width = tokens.shape[1]
    depth = rows * n_fs
    units = depth // n_tp

    cfg = Config()
    cfg.dims = dims
    cfg.inner = 2 if n_fs % 2 == 0 else 1
    cfg.nz = n_fs // cfg.inner
    part = tok_count // n_tp
    cfg.R = R = -(-part // 16) * 16
    cfg.CT = min(256, cols)
    cfg.NT = width // cfg.CT
    cfg.NB = min(256, depth)
    cfg.extra = extra = -(-2 * count // 128) * 128

    values = tokens.astype(F32)
    normed = (values * lax.rsqrt(jnp.mean(values * values, axis=-1, keepdims=True) + EPS)).astype(BF)
    named = routes[:, :, None] == jnp.arange(count, dtype=jnp.int32)[None, None, :]
    weight = jnp.sum(jnp.where(named, route_weight[:, :, None], 0.0), axis=1)
    high = lax.reduce_precision(weight, 8, 7)
    tail = jnp.concatenate(
        [high.astype(BF), (weight - high).astype(BF), jnp.zeros((tok_count, extra - 2 * count), BF)], axis=1)

    def in_parts(a):
        a = a.reshape(n_tp, part, a.shape[-1])
        return jnp.pad(a, ((0, 0), (0, R - part), (0, 0)))
    local = in_parts(normed)
    rows_here = lax.dynamic_index_in_dim(
        jnp.concatenate([local, in_parts(tail)], axis=2), tp_index, 0, keepdims=False)
    local = local.reshape(n_tp * R, width)

    gain_shared = lax.dynamic_slice_in_dim(
        norm_gain, fs_index * gate_shared.shape[0], gate_shared.shape[0], 0)
    gs = (gate_shared * gain_shared[:, None]).astype(BF)
    us = (up_shared * gain_shared[:, None]).astype(BF)
    dsh = down_shared.astype(BF)
    gain_cols = lax.dynamic_slice_in_dim(norm_gain, tp_index * cols, cols, 0)
    gate = (gate_experts[0] * gain_cols[None, None, :]).astype(BF)
    upper = (up_experts[0] * gain_cols[None, None, :]).astype(BF)
    down = down_experts[0].astype(BF)
    cfg.parts = tuple(n_gr if a.shape[0] % (16 * n_gr) == 0 else 1 for a in (gs, us, dsh))

    nz, inner, NT, CT = cfg.nz, cfg.inner, cfg.NT, cfg.CT
    tiles = NT // n_tp
    sds = jax.ShapeDtypeStruct
    outs = (
        sds((n_tp, R, cols), BF),
        sds((n_gr, 1, units, width), BF),
        sds((n_gr, 1, units, width), BF),
        sds((n_gr, 1, depth, cols), BF),
        sds((n_fs * gs.shape[0], gs.shape[1]), BF),
        sds((n_fs * us.shape[0], us.shape[1]), BF),
        sds((n_fs * dsh.shape[0], dsh.shape[1]), BF),
    )
    V, DMA = pltpu.VMEM, pltpu.SemaphoreType.DMA
    q, p, r = max(1, n_tp - 1), max(1, n_gr - 1), max(1, inner - 1)
    scratch = [
        V((n_fs * R, width + extra), BF),
        V((3, n_gr, depth, width), BF),
        V((n_fs * R, n_gr * depth), BF),
        V(outs[4].shape, BF), V(outs[5].shape, BF), V(outs[6].shape, BF),
        V((n_tp, n_tp * R, gs.shape[1]), BF),
        V((n_tp * R, cols), F32),
        V((NT, r, nz * R, CT), BF), V((NT, r, nz * R, CT), BF),
        V((NT, nz * R, CT), F32),
        V((2, NT, nz * R, CT), BF), V((2, NT, nz * R, CT), BF),
        V((NT, R, CT), BF), V((n_tp, tiles, R, CT), BF),
        DMA((3,)), DMA((3, n_fs)), DMA((3,)), DMA((3, q)), DMA((3, q)),
        DMA((3, n_tp, p)), DMA((3, n_tp, p)),
        DMA((4, 2, nz)), DMA((4, 2, nz)), DMA((4, r, 2 * nz - 1)), DMA((4, r, 2 * nz - 1)),
        DMA((4,)), DMA((4, p)), DMA((4, p)),
        DMA((q,)), DMA((q,)), DMA((NT, r)), DMA((NT, r)), DMA((2, NT)), DMA((2, NT)),
        DMA((NT,)), DMA((n_tp, tiles)), DMA((6, n_gr)),
    ]
    anyw = pl.BlockSpec(memory_space=pl.ANY)
    vmem = pl.BlockSpec(memory_space=pltpu.VMEM)
    mixed, gate_w, up_w, down_w, gs_w, us_w, ds_w = pl.pallas_call(
        functools.partial(whole, cfg),
        out_shape=outs,
        in_specs=[anyw, vmem] + [anyw] * 6,
        out_specs=(vmem,) + (anyw,) * 6,
        scratch_shapes=scratch,
        compiler_params=pltpu.CompilerParams(
            collective_id=1, has_side_effects=True, vmem_limit_bytes=60 << 20),
        cost_estimate=pl.CostEstimate(flops=0, bytes_accessed=200 << 20, transcendentals=0),
    )(rows_here, local, gate, upper, down, gs, us, dsh)
    mixed = mixed[:, :part].reshape(tok_count, cols)
    return (mixed, gate_w, up_w, down_w, gs_w, us_w, ds_w)


def solution(mesh):
    return jax.shard_map(
        on_device,
        mesh=mesh,
        in_specs=(
            P(("gr", "fs"), None),
            P(("gr", "fs"), None),
            P(("gr", "fs"), None),
            P(),
            P("gr", None, "fs", "tp"),
            P("gr", None, "fs", "tp"),
            P("gr", None, "fs", "tp"),
            P("fs", "tp"),
            P("fs", "tp"),
            P("fs", "tp"),
        ),
        out_specs=(
            P(("gr", "fs"), "tp"),
            P(None, "fs", "tp", None),
            P(None, "fs", "tp", None),
            P(None, "fs", None, "tp"),
            P(None, "tp"),
            P(None, "tp"),
            P(None, "tp"),
        ),
        check_vma=False,
    )
```

time: 316 us -> 223 us (0.71)
  waiting for transfers between devices: 63.5 us -> 0 us
  matrix products: 29.6 us -> 0 us
  Pallas kernels: 176 us -> 194 us
  between operations: 14.3 us -> 0.7 us
  blocking collectives: 5.29 us -> 0 us
  local copies, waits for them, and re-layouts: 13.1 us -> 17.1 us
  other arithmetic: 14.1 us -> 10.4 us
    reduce_scatter x1 -> x0, waiting for transfers between devices: 63.4 us -> none  [on_device(): routed = lax.psum_scatter(partial, 'fs', scatter_dimension=0, tiled=True)]
    dot_general x11 -> x0, matrix products: 29.6 us -> none  [the longest x2 9.16 us: on_device(): lax.dot_general(x, gate_w[g, k], (((1,), (1,)), ((), ())), preferred_elem...]
    pallas_call x2 -> x1, Pallas kernels: 176 us -> 194 us  [on_device(): pl.pallas_call(functools.partial(whole, cfg), out_shape=outs, in_specs=[a...]
    all_gather x1 -> x0, blocking collectives: 5.29 us -> none  [on_device(): shared_full = lax.all_gather(shared_hidden, 'tp', axis=1, tiled=True)]
    unnamed x44 -> x25, local copies, waits for them, and re-layouts: 10.7 us -> 12.9 us
  transfers between devices with their start and end apart: 2 -> 0, of which waited for: 1 -> 0; matrix products, arithmetic and copies ran while one was open for 1% -> 0% of each run, Pallas kernels for 17% -> 0%
where the time goes in v1:
time: 223 us; the launch traced here: 222 us
  Pallas kernels  194 us (87%)
  local copies, waits for them, and re-layouts  17.1 us (8%)
  other arithmetic  10.4 us (5%)
    pallas_call x1, Pallas kernels, on_device(): pl.pallas_call(functools.partial(whole, cfg), out_shape=outs, in_specs=[a...  194 us
    unnamed x25, local copies, waits for them, and re-layouts  12.9 us

profile of v1, /device:TPU:0, one launch (start us, length us, event | category | flops | bytes accessed | tf_op | source)
XLA Modules:
  0.0 222.2 jit_solution(15710205157026023215)
XLA Ops:
  0.6 0.0 copy-start.1
  0.7 0.8 dynamic_slice.12
  1.5 1.4 fusion.2
  2.9 0.7 select_reduce_fusion
  3.6 0.1 reduce_sum.22
  3.7 0.1 copy.26
  3.8 0.1 copy.25
  3.9 1.6 convert_element_type.44.ds_l
  5.6 1.8 multiply_convert_fusion
  7.4 0.0 copy-done.1
  7.4 0.2 fusion.3.local_in
  7.6 0.0 copy-start
  7.6 0.0 copy-start.2
  7.6 1.1 concatenate.6
  8.7 1.9 dynamic-slice_bitcast_fusion.rows_in
  10.6 0.0 copy-done.2
  10.6 1.1 convert_bitcast_fusion.down_l
  11.8 0.0 copy-done
  11.8 0.0 dynamic-slice-done
  11.8 3.5 %fusion = (bf16[8,64,1024]{2,1,0:T(8,128)(2,1)}, bf16[8,64,1024]{2,1,0:T(8,128)(2,1)}) fusion(f32[1,8,64,1024]{3,2,1,0:T(8,128)S(1)} %copy-done.5, f32[1024]{0:T(1024)S(1)} %dynamic-slice-done, f32[1,8,64,1024]{3,2,1,0:T(8,128)} %param.14), kind=kLoop, calls=%fused_computation.1 | loop fusion | flops 2097152 | bytes 6295552 | tf_op jit(solution)/shard_map/convert_element_type | solution.py:541
  15.3 194.0 %shard_map.153 = (bf16[2,96,1024]{2,1,0:T(8,128)(2,1)}, bf16[2,1,256,2048]{3,2,1,0:T(8,128)(2,1)}, bf16[2,1,256,2048]{3,2,1,0:T(8,128)(2,1)}, bf16[2,1,512,1024]...) custom-call(bf16[96,2176]{1,0:T(8,128)(2,1)} %dynamic-slice_bitcast_fusion.r, ...), custom_call_target="tpu_custom_call" | custom-call | bytes 209715200 | tf_op jit(solution)/shard_map/pallas_call | solution.py:579
  209.3 1.8 copy.36
  211.1 3.3 %copy.37 = bf16[2,1,256,2048]{3,2,1,0:T(8,128)(2,1)} copy(bf16[2,1,256,2048]{3,2,1,0:T(8,128)(2,1)} %get-tuple-element.35) | data formatting | bytes 4194304
  214.4 1.3 copy.38
  215.7 1.0 copy-done.3
  216.7 1.3 copy.39
  218.1 0.6 copy-done.8
  218.7 1.0 copy.40
  219.7 0.6 copy-done.7
  220.3 1.0 copy.41
  221.3 0.0 copy-done.6
  221.3 1.0 copy.42
  (12 shorter events, 0.0 us)
Async XLA Ops:
  0.6 6.8 %copy-start.1 = (bf16[192,2048]{1,0:T(8,128)(2,1)S(1)}, bf16[192,2048]{1,0:T(8,128)(2,1)}, u32[]{:S(2)}) copy-start(bf16[192,2048]{1,0:T(8,128)(2,1)} %param.10) | copy-start | bytes 2359300
  7.6 4.2 %copy-start = (bf16[192,2048]{1,0:T(8,128)(2,1)}, bf16[192,2048]{1,0:T(8,128)(2,1)S(1)}, u32[]{:S(2)}) copy-start(bf16[192,2048]{1,0:T(8,128)(2,1)S(1)} %fusion.3.local_in) | copy-start | bytes 2359300
  7.6 3.0 %copy-start.2 = (f32[1,8,64,1024]{3,2,1,0:T(8,128)S(1)}, f32[1,8,64,1024]{3,2,1,0:T(8,128)}, u32[]{:S(2)}) copy-start(f32[1,8,64,1024]{3,2,1,0:T(8,128)} %param.16) | copy-start | bytes 6291460
  8.7 3.1 %copy-start.5 = (f32[1,8,64,1024]{3,2,1,0:T(8,128)S(1)}, f32[1,8,64,1024]{3,2,1,0:T(8,128)}, u32[]{:S(2)}) copy-start(f32[1,8,64,1024]{3,2,1,0:T(8,128)} %param.15) | copy-start | bytes 6291460
  8.7 3.1 %dynamic-slice-start = ((f32[2048]{0:T(1024)}, s32[]{:T(128)}), f32[1024]{0:T(1024)S(1)}, s32[]{:S(2)}) async-start(f32[2048]{0:T(1024)} %param.13, s32[]{:T(128)} %select_n.16), calls=%async_computation | async-start | bytes 8704 | tf_op jit(solution)/shard_map/dynamic_slice | solution.py:539
  211.1 3.3 %copy-start.4 = (bf16[2,1,256,2048]{3,2,1,0:T(8,128)(2,1)S(1)}, bf16[2,1,256,2048]{3,2,1,0:T(8,128)(2,1)}, u32[]{:S(2)}) copy-start(bf16[2,1,256,2048]{3,2,1,0:T(8,128)(2,1)} %get-tuple-element.36) | copy-start | bytes 6291460
  214.4 2.3 %copy-start.3 = (bf16[2,1,512,1024]{3,2,1,0:T(8,128)(2,1)S(1)}, bf16[2,1,512,1024]{3,2,1,0:T(8,128)(2,1)}, u32[]{:S(2)}) copy-start(bf16[2,1,512,1024]{3,2,1,0:T(8,128)(2,1)} %get-tuple-element.37) | copy-start | bytes 6291460
  216.7 2.0 copy-start.8
  218.7 1.6 copy-start.7
  218.7 2.6 %copy-start.6 = (bf16[512,1024]{1,0:T(8,128)(2,1)S(1)}, bf16[512,1024]{1,0:T(8,128)(2,1)}, u32[]{:S(2)}) copy-start(bf16[512,1024]{1,0:T(8,128)(2,1)} %get-tuple-element.40) | copy-start | bytes 3145732

commit v2 on v1

v2 whole, which is shorter than its diff:
```python
import functools

import jax
import jax.numpy as jnp
from jax import lax
from jax.experimental import pallas as pl
from jax.experimental.pallas import tpu as pltpu
from jax.sharding import PartitionSpec as P

EPS = 1e-06
MESH = pl.DeviceIdType.MESH
BF = jnp.bfloat16
F32 = jnp.float32


def whole(cfg, tok_in, route_in, weight_in, gain_in, gate_in, up_in, down_in, gs_in, us_in, ds_in,
          mixed_o, gate_o, up_o, down_o, gs_o, us_o, ds_o,
          X, W, H, GS, US, DS, SH, SO, PS, YR, S, ZS, ZR, FS, FR, ST, LB, LG, LU, LD, LN,
          st_sem, b_send, b_recv, b_own, x_send, x_recv, p_send, p_recv,
          c_zs, c_zr, c_ys, c_yr, c_own, g_send, g_recv,
          sh_send, sh_recv, y_send, y_recv, z_send, z_recv, f_send, f_recv, o_sem):
    n_gr, n_fs, n_tp = cfg.dims
    inner, nz, R, NT, CT, DG = cfg.inner, cfg.nz, cfg.R, cfg.NT, cfg.CT, cfg.DG
    gr, fs, tp = lax.axis_index("gr"), lax.axis_index("fs"), lax.axis_index("tp")
    z, y = fs // inner, fs % inner
    rows, cols = gate_in.shape[1], gate_in.shape[2]
    width = cols * n_tp
    depth = rows * n_fs
    units = depth // n_tp
    count = n_gr * n_fs
    half = nz * R

    def ds(start, size):
        if isinstance(start, int):
            return pl.ds(start, size)
        return pl.ds(pl.multiple_of(start * 1, size), size)

    def remote(src, dst, s, r, to):
        return pltpu.make_async_remote_copy(
            src_ref=src, dst_ref=dst, send_sem=s, recv_sem=r, device_id=to, device_id_type=MESH)

    barrier = pltpu.get_barrier_semaphore()

    def greet(d, c):
        pl.semaphore_signal(barrier, inc=1, device_id=(gr, (fs + d) % n_fs, tp), device_id_type=MESH)
        return c
    lax.fori_loop(1, n_fs, greet, 0)
    for q in range(1, n_tp):
        pl.semaphore_signal(barrier, inc=1, device_id=(gr, fs, (tp + q) % n_tp), device_id_type=MESH)
    for p in range(1, n_gr):
        pl.semaphore_signal(barrier, inc=1, device_id=((gr + p) % n_gr, fs, tp), device_id_type=MESH)

    def stage(m):
        return pltpu.make_async_copy((gate_in, up_in, down_in)[m], ST.at[m % 2], st_sem.at[m])
    stage(0).start()
    stage(1).start()

    def normalize(i, c):
        at_rows = ds(i * 16, 16)
        v = tok_in[at_rows, :].astype(F32)
        v = v * lax.rsqrt(jnp.mean(v * v, axis=-1, keepdims=True) + EPS)
        LN[at_rows, :] = v.astype(BF)
        return c
    lax.fori_loop(0, n_tp * R // 16, normalize, 0)
    mine = ds(tp * R, R)
    X[ds(z * R, R), pl.ds(0, width)] = LN[mine, :]
    named, shares = route_in[mine, :], weight_in[mine, :]
    lane = lax.broadcasted_iota(jnp.int32, (R, cfg.extra), 1)
    tail = jnp.zeros((R, cfg.extra), F32)
    for j in range(named.shape[1]):
        e, w = named[:, j:j + 1], shares[:, j:j + 1]
        high = w.astype(BF).astype(F32)
        tail = tail + jnp.where(lane == e, high, 0.0) + jnp.where(lane == e + count, w - high, 0.0)
    X[ds(z * R, R), pl.ds(width, cfg.extra)] = tail.astype(BF)

    gain = gain_in[:, ds(tp * cols, cols)]

    def convert(m):
        stage(m).wait()

        def one(k, c):
            v = ST[m % 2, k]
            LB[m, k] = (v * gain if m < 2 else v).astype(BF)
            return c
        lax.fori_loop(0, n_fs, one, 0)
    convert(0)
    stage(2).start()

    gw = cols // DG

    def span(m):
        return (0, cols) if m < 2 else ((m - 2) * gw, gw)

    def block(m, s, t):
        lo, size = span(m)
        return W.at[min(m, 2), gr, ds(s * rows, rows), pl.ds(pl.multiple_of(t * cols + lo, size), size)]

    def region(m, g, t):
        lo, size = span(m)
        return W.at[min(m, 2), g, :, pl.ds(pl.multiple_of(t * cols + lo, size), size)]

    def local(m, k):
        lo, size = span(m)
        return LB.at[min(m, 2), k, :, pl.ds(lo, size)]

    def to_expert(m, k):
        return remote(local(m, k), block(m, fs, tp), b_send.at[m], b_recv.at[m, fs], (gr, k, tp))

    def own_block(m):
        return pltpu.make_async_copy(local(m, fs), block(m, fs, tp), b_own.at[m])

    def each_other(act, lo=1, hi=n_fs):
        def step(d, c):
            pl.when(fs + d < n_fs)(lambda: act(fs + d))
            pl.when(fs - d >= 0)(lambda: act(fs - d))
            return c
        lax.fori_loop(lo, hi, step, 0)

    def across(m, src, s):
        for q in range(1, n_tp):
            remote(src, block(m, s, tp), x_send.at[m, q - 1], x_recv.at[m, q - 1],
                   (gr, fs, (tp + q) % n_tp)).start()

    def keep_own(m):
        own_block(m).start()
        across(m, local(m, fs), fs)

    def send(m, k):
        to_expert(m, k).start()

    def landed(m, s):
        part = block(m, s, tp)
        remote(part, part, b_recv.at[m, s], b_recv.at[m, s], (gr, s, tp)).wait_recv()
        across(m, part, s)

    def partner(m, g, q, p):
        part = region(m, g, (tp + n_tp - q) % n_tp)
        return remote(part, part, p_send.at[m, q, p - 1], p_recv.at[m, q, p - 1],
                      ((gr + p) % n_gr, fs, tp))

    def share(m, q):
        for p in range(1, n_gr):
            partner(m, gr, q, p).start()

    def shared_landed(m, q):
        for p in range(1, n_gr):
            partner(m, (gr + n_gr - p) % n_gr, q, p).wait_recv()

    def x_landed(m, q):
        part = region(m, gr, (tp + n_tp - q) % n_tp)
        remote(part, part, x_send.at[m, q - 1], x_recv.at[m, q - 1],
               (gr, fs, (tp + q) % n_tp)).wait_recv()

    def token_place(zz, yr):
        return X.at[ds((yr * nz + zz) * R, R), :]

    def shared_item(src, dst, parts):
        size = src.shape[0] // parts

        def place(zz, yr):
            f = zz * inner + (y + yr) % inner
            if parts == 1:
                return dst.at[ds(f * size, size), :]
            return dst.at[ds((f * parts + gr) * size, size), :]
        return (src if parts == 1 else src.at[ds(gr * size, size), :], place, parts)
    items = ((token_place(z, 0), token_place, 1),) + tuple(
        shared_item(s, d, p) for s, d, p in zip((LG, LU, LD), (GS, US, DS), cfg.parts))

    def at(way, d):
        return z - d if way == 0 else z + d

    def z_copy(m, way, d):
        own, place, _ = items[m]
        dst = place(at(way, d), 0)
        return remote(own if d == 0 else dst, dst, c_zs.at[m, way, d], c_zr.at[m, way, d],
                      (gr, (z + 1 if way == 0 else z - 1) * inner + y, tp))

    def y_slot(d, way):
        return d + way * (nz - 1) if d else 0

    def y_copy(m, q, way, d):
        own, place, parts = items[m]
        zz = at(way, d)
        src = own if d == 0 else place(zz, 0)
        dst = place(zz, inner - q) if m == 0 else place(zz, 0)
        i = y_slot(d, way)
        return remote(src, dst, c_ys.at[m, q - 1, i], c_yr.at[m, q - 1, i],
                      (gr, z * inner + (y + q) % inner, tp))

    def pass_partner(m, part):
        if items[m][2] > 1:
            for p in range(1, n_gr):
                remote(part, part, g_send.at[m, p - 1], g_recv.at[m, p - 1],
                       ((gr + p) % n_gr, fs, tp)).start()

    def next_there(way):
        return (z < nz - 1) if way == 0 else (z > 0)

    def there(d, way):
        return (z - d >= 0) if way == 0 else (z + d < nz)

    def gather_start(m):
        own, place, parts = items[m]
        for way in (0, 1):
            pl.when(next_there(way))(lambda way=way: z_copy(m, way, 0).start())
        for q in range(1, inner):
            y_copy(m, q, 0, 0).start()
        if m:
            pltpu.make_async_copy(own, place(z, 0), c_own.at[m]).start()

    def gather_own(m):
        own, place, parts = items[m]
        pltpu.make_async_copy(own, place(z, 0), c_own.at[m]).wait()
        pass_partner(m, place(z, 0))

    def gather_pass(m, d):
        for way in (0, 1):
            def act(way=way):
                part = items[m][1](at(way, d), 0)
                remote(part, part, c_zs.at[m, way, d - 1], c_zr.at[m, way, d - 1],
                       (gr, (z + 1 if way == 0 else z - 1) * inner + y, tp)).wait_recv()
                if d < nz - 1:
                    pl.when(next_there(way))(lambda: z_copy(m, way, d).start())
                for q in range(1, inner):
                    y_copy(m, q, way, d).start()
                pass_partner(m, part)
            pl.when(there(d, way))(act)

    places = [(0, 0)] + [(d, way) for d in range(1, nz) for way in (0, 1)]

    def gather_y(m):
        for d, way in places:
            def act(d=d, way=way):
                for q in range(1, inner):
                    part = items[m][1](at(way, d), inner - q)
                    i = y_slot(d, way)
                    remote(part, part, c_ys.at[m, q - 1, i], c_yr.at[m, q - 1, i],
                           (gr, z * inner + (y + q) % inner, tp)).wait_recv()
                    pass_partner(m, part)
            if d == 0:
                act()
            else:
                pl.when(there(d, way))(act)

    def gather_sent(m):
        for d, way in places:
            def act(d=d, way=way):
                for w in ((0, 1) if d == 0 else (way,)):
                    if d < nz - 1:
                        pl.when(next_there(w))(lambda w=w: z_copy(m, w, d).wait_send())
                for q in range(1, inner):
                    y_copy(m, q, way, d).wait_send()
            if d == 0:
                act()
            else:
                pl.when(there(d, way))(act)

    def partner_gathered(m, way):
        dst = (X, GS, US, DS)[m]
        if items[m][2] > 1:
            part = dst.at[pl.ds(0, dst.shape[0] // items[m][2]), :]
            for p in range(1, n_gr):
                c = remote(part, part, g_send.at[m, p - 1], g_recv.at[m, p - 1],
                           ((gr + p) % n_gr, fs, tp))
                if way:
                    c.wait_send()
                else:
                    c.wait_recv()

    per = depth // CT
    chunks = n_gr * per
    lanes = lax.broadcasted_iota(jnp.int32, (n_fs * R, cfg.extra), 1)
    dn = (((1,), (1,)), ((), ()))

    def gate_product(i, c):
        gg, n = (gr + i // per) % n_gr, i % per
        v = lax.dot_general(X[:, pl.ds(0, width)], W[0, gg, ds(n * CT, CT), :], dn,
                            preferred_element_type=F32)
        for r in range(inner):
            S[i * inner + r] = v[r * half:(r + 1) * half]
        return c

    def up_product(i, c):
        gg, n = (gr + i // per) % n_gr, i % per
        v = lax.dot_general(X[:, pl.ds(0, width)], W[1, gg, ds(n * CT, CT), :], dn,
                            preferred_element_type=F32)
        expert = gg * n_fs + fs
        pick = (lanes == expert) | (lanes == count + expert)
        weight = jnp.sum(jnp.where(pick, X[:, pl.ds(width, cfg.extra)].astype(F32), 0.0),
                         axis=1, keepdims=True)
        for r in range(inner):
            part = slice(r * half, (r + 1) * half)
            gate = S[i * inner + r]
            H[pl.ds(r * half, half), ds((gg * per + n) * CT, CT)] = (
                gate / (1.0 + jnp.exp(-gate)) * v[part] * weight[part]).astype(BF)
        return c

    pl.semaphore_wait(barrier, n_fs - 1 + n_tp - 1 + n_gr - 1)
    stops = max(1, nz - 1)
    size = -(-(n_fs - 1) // stops)
    parts = [(1 + k * size, min(n_fs, 1 + (k + 1) * size)) for k in range(stops)]
    gather_start(0)
    keep_own(0)
    each_other(lambda k: send(0, k), *parts[0])
    convert(1)
    keep_own(1)
    at_row = lax.broadcasted_iota(jnp.int32, (LG.shape[0], width), 0) + fs * LG.shape[0]
    at_col = lax.broadcasted_iota(jnp.int32, (LG.shape[0], width), 1)
    gain_rows = jnp.sum(jnp.where(at_row == at_col, gain_in[...], 0.0), axis=1, keepdims=True)
    LG[...] = (gs_in[...] * gain_rows).astype(BF)
    LU[...] = (us_in[...] * gain_rows).astype(BF)
    LD[...] = ds_in[...].astype(BF)
    convert(2)
    if nz > 1:
        gather_pass(0, 1)
    for part in parts[1:]:
        each_other(lambda k: send(0, k), *part)

    def second(s):
        landed(1, s)
        send(2, s)
    for k, part in enumerate(parts):
        each_other(lambda s: landed(0, s), *part)
        if k + 2 < nz - 1 or k + 2 == nz - 1 == 2:
            gather_pass(0, k + 2)
        each_other(lambda s: send(1, s), *part)
    own_block(0).wait()
    share(0, 0)
    for m in range(2, 2 + DG):
        keep_own(m)
    for m in (1, 2, 3):
        gather_start(m)
    for k, part in enumerate(parts):
        each_other(second, *part)
        if k == 0:
            if nz > 3:
                gather_pass(0, nz - 1)
            for m in (1, 2, 3):
                gather_own(m)
            for q in range(1, n_tp):
                x_landed(0, q)
                share(0, q)
        if k == max(0, stops - 2):
            gather_y(0)
            lax.fori_loop(0, per, gate_product, 0)
    shared_pass = [(lambda d=d: [gather_pass(m, d) for m in (1, 2, 3)]) for d in range(1, nz)]
    for d in range(0, max(0, nz - 3)):
        shared_pass[d]()
    for m in range(3, 2 + DG):
        each_other(lambda k: send(m, k))
    own_block(1).wait()
    share(1, 0)
    for q in range(n_tp):
        shared_landed(0, q)
    lax.fori_loop(per, chunks, gate_product, 0)
    for q in range(1, n_tp):
        x_landed(1, q)
        share(1, q)
    for d in range(max(0, nz - 3), max(0, nz - 2)):
        shared_pass[d]()

    def out_wide(m, g):
        return pltpu.make_async_copy(
            W.at[m, g, ds(tp * units, units), :], (gate_o, up_o)[m].at[g, 0], o_sem.at[m, g])

    def out_tall(g):
        return pltpu.make_async_copy(
            W.at[2, g, :, ds(tp * cols, cols)], down_o.at[g, 0], o_sem.at[2, g])

    for g in range(n_gr):
        out_wide(0, g).start()

    each = -(-(n_fs - 1) // chunks)

    def ahead(i, c):
        up_product(i, 0)
        each_other(lambda s: landed(2, s), 1 + i * each, jnp.minimum(n_fs, 1 + (i + 1) * each))
        return c
    lax.fori_loop(0, per, ahead, 0)
    for q in range(n_tp):
        shared_landed(1, q)
    for g in range(n_gr):
        out_wide(1, g).start()
    for d in range(max(0, nz - 2), nz - 1):
        shared_pass[d]()
    lax.fori_loop(per, chunks, ahead, 0)

    tiles = NT // n_tp
    each_group = tiles // DG
    group = n_tp * each_group

    def owner(i):
        return (tp + i // each_group % n_tp) % n_tp

    def place_in(i):
        return i // group * each_group + i % each_group

    def y_out(i, r):
        return remote(PS.at[i, r - 1], YR.at[i, r - 1], y_send.at[i, r - 1], y_recv.at[i, r - 1],
                      (gr, z * inner + (y + r) % inner, tp))

    def produce(i, c):
        at_cols = ds((owner(i) * tiles + place_in(i)) * CT, CT)
        part = jnp.zeros((n_fs * R, CT), F32)
        for g in range(n_gr):
            part = part + jnp.dot(H[:, pl.ds(g * depth, depth)], W[2, g, :, at_cols],
                                  preferred_element_type=F32)
        S[i] = part[:half]
        for r in range(1, inner):
            PS[i, r - 1] = part[r * half:(r + 1) * half].astype(BF)

        @pl.when(i % each_group > 0)
        def _():
            for r in range(1, inner):
                y_out(i - 1, r).start()
        return c

    def tell(i):
        for r in range(1, inner):
            y_out(i, r).start()

    def make(a, u):
        m = 2 + a
        if u:
            x_landed(m, u)
        else:
            own_block(m).wait()
        share(m, u)
        shared_landed(m, u)
        base = (a * n_tp + (n_tp - u) % n_tp) * each_group
        lax.fori_loop(base, base + each_group, produce, 0)
        tell(base + each_group - 1)

    turn = [0] + [n_tp - u for u in range(1, n_tp)]
    for u in turn:
        make(0, u)

    for m in (1, 2, 3):
        gather_y(m)
        partner_gathered(m, 0)
    sg = jnp.dot(LN[...], GS[...], preferred_element_type=F32)
    su = jnp.dot(LN[...], US[...], preferred_element_type=F32)
    SH[tp] = (sg / (1.0 + jnp.exp(-sg)) * su).astype(BF)
    shared_outs = [pltpu.make_async_copy(a, b, o_sem.at[3 + i, 0])
                   for i, (a, b) in enumerate(((GS, gs_o), (US, us_o), (DS, ds_o)))]
    for c in shared_outs:
        c.start()

    def sh_copy(q):
        return remote(SH.at[tp], SH.at[tp], sh_send.at[q - 1], sh_recv.at[q - 1],
                      (gr, fs, (tp + q) % n_tp))
    for q in range(1, n_tp):
        sh_copy(q).start()

    def shared_rest():
        for q in range(1, n_tp):
            part = SH.at[(tp + n_tp - q) % n_tp]
            remote(part, part, sh_send.at[q - 1], sh_recv.at[q - 1], (gr, fs, (tp + q) % n_tp)).wait_recv()
        total = jnp.zeros((n_tp * R, cols), F32)
        su_n = GS.shape[1]
        for t in range(n_tp):
            total = total + jnp.dot(SH[t], DS[pl.ds(t * su_n, su_n), :], preferred_element_type=F32)
        SO[...] = total

    def z_move(way, i, lo, size, to):
        return remote(ZS.at[way, i, pl.ds(lo, size), :], ZR.at[way, i, pl.ds(lo, size), :],
                      z_send.at[way, i], z_recv.at[way, i], (gr, to * inner + y, tp))

    def upward(i, h):
        lo, size = (h + 1) * R, (nz - 1 - h) * R
        if h > 0:
            z_move(0, i, h * R, (nz - h) * R, z + 1).wait_recv()
            S[i, pl.ds(h * R, R), :] = S[i, pl.ds(h * R, R), :] + ZR[0, i, pl.ds(h * R, R), :].astype(F32)
            ZS[0, i, pl.ds(lo, size), :] = (
                S[i, pl.ds(lo, size), :] + ZR[0, i, pl.ds(lo, size), :].astype(F32)).astype(BF)
        else:
            ZS[0, i, pl.ds(lo, size), :] = S[i, pl.ds(lo, size), :].astype(BF)
        z_move(0, i, lo, size, z + 1).start()

    def downward(i, h):
        zz = nz - 1 - h
        size = zz * R
        if h > 0:
            z_move(1, i, 0, size + R, z - 1).wait_recv()
            S[i, pl.ds(size, R), :] = S[i, pl.ds(size, R), :] + ZR[1, i, pl.ds(size, R), :].astype(F32)
            ZS[1, i, pl.ds(0, size), :] = (
                S[i, pl.ds(0, size), :] + ZR[1, i, pl.ds(0, size), :].astype(F32)).astype(BF)
        else:
            ZS[1, i, pl.ds(0, size), :] = S[i, pl.ds(0, size), :].astype(BF)
        z_move(1, i, 0, size, z - 1).start()

    def f_copy(i):
        return remote(FS.at[i], FR.at[tp, place_in(i)], f_send.at[i], f_recv.at[tp, place_in(i)],
                      (gr, fs, owner(i)))

    def is_mine(i):
        return i // each_group % n_tp == 0

    def finish(i):
        if nz > 1:
            last = (nz - 1) * R

            @pl.when(z == nz - 1)
            def _():
                z_move(0, i, last, R, z - 1).wait_recv()
                S[i, pl.ds(last, R), :] = S[i, pl.ds(last, R), :] + ZR[0, i, pl.ds(last, R), :].astype(F32)

            @pl.when(z == 0)
            def _():
                z_move(1, i, 0, R, z + 1).wait_recv()
                S[i, pl.ds(0, R), :] = S[i, pl.ds(0, R), :] + ZR[1, i, pl.ds(0, R), :].astype(F32)
        done = S[i, ds(z * R, R), :]

        @pl.when(is_mine(i))
        def _():
            at_cols = ds(place_in(i) * CT, CT)
            mixed_o[tp, :, at_cols] = (done + SO[ds(tp * R, R), at_cols]).astype(BF)

        @pl.when(jnp.logical_not(is_mine(i)))
        def _():
            FS[i] = done.astype(BF)
            f_copy(i).start()

    turns = 3 if DG > 1 else 0
    some = -(-(n_fs - 1) // 3)

    def advance(j, c):
        if DG > 1:
            @pl.when(j < turns)
            def _():
                each_other(lambda s: landed(3, s), jnp.minimum(n_fs, 1 + j * some),
                           jnp.minimum(n_fs, 1 + (j + 1) * some))
            for k, u in enumerate(turn):
                pl.when(j == turns + k)(lambda u=u: make(1, u))
        pl.when(j == min(2, max(0, nz - 2)))(shared_rest)

        @pl.when(j < NT)
        def _():
            for r in range(1, inner):
                part = YR.at[j, r - 1]
                remote(part, part, y_send.at[j, r - 1], y_recv.at[j, r - 1],
                       (gr, z * inner + (y + r) % inner, tp)).wait_recv()
            S[j] = S[j] + sum([YR[j, r - 1].astype(F32) for r in range(1, inner)], 0.0)
        for h in range(nz - 1):
            i = j - h

            @pl.when((i >= 0) & (i < NT))
            def _(i=i, h=h):
                pl.when(z == h)(lambda: upward(i, h))
                pl.when(z == nz - 1 - h)(lambda: downward(i, h))
        i = j - (nz - 1)
        pl.when(i >= 0)(lambda: finish(i))
        return c
    lax.fori_loop(0, NT + nz - 1, advance, 0)
    for g in range(n_gr):
        out_tall(g).start()

    def arrive(i, c):
        for q in range(1, n_tp):
            t = (tp + n_tp - q) % n_tp
            part = FR.at[t, i]
            remote(part, part, f_send.at[0], f_recv.at[t, i], (gr, fs, t)).wait_recv()
            at_cols = ds(i * CT, CT)
            mixed_o[t, :, at_cols] = (FR[t, i].astype(F32) + SO[ds(t * R, R), at_cols]).astype(BF)
        return c
    lax.fori_loop(0, tiles, arrive, 0)

    for m in range(2 + DG):
        lo, size_m = span(m)
        part = LB.at[min(m, 2), pl.ds(0, n_fs - 1), :, pl.ds(lo, size_m)]
        remote(part, part, b_send.at[m], b_send.at[m], (gr, fs, (tp + 1) % n_tp)).wait_send()
        for q in range(1, n_tp):
            part = region(m, gr, tp)
            remote(part, part, x_send.at[m, q - 1], x_recv.at[m, q - 1],
                   (gr, fs, (tp + q) % n_tp)).wait_send()
        for q in range(n_tp):
            for p in range(1, n_gr):
                partner(m, gr, q, p).wait_send()
    for m in range(4):
        gather_sent(m)
        partner_gathered(m, 1)
    for q in range(1, n_tp):
        sh_copy(q).wait_send()

    def drain(i, c):
        for r in range(1, inner):
            y_out(i, r).wait_send()
        for h in range(nz - 1):
            pl.when(z == h)(lambda h=h: z_move(0, i, (h + 1) * R, (nz - 1 - h) * R, z + 1).wait_send())
            pl.when(z == nz - 1 - h)(lambda h=h: z_move(1, i, 0, (nz - 1 - h) * R, z - 1).wait_send())
        pl.when(jnp.logical_not(is_mine(i)))(lambda: f_copy(i).wait_send())
        return c
    lax.fori_loop(0, NT, drain, 0)
    for g in range(n_gr):
        out_tall(g).wait()
        for m in (0, 1):
            out_wide(m, g).wait()
    for c in shared_outs:
        c.wait()


class Config:
    pass


def on_device(tokens, routes, route_weight, norm_gain, gate_experts, up_experts, down_experts,
              gate_shared, up_shared, down_shared):
    dims = (lax.axis_size("gr"), lax.axis_size("fs"), lax.axis_size("tp"))
    n_gr, n_fs, n_tp = dims
    per_group, rows, cols = gate_experts.shape[1:]
    count = per_group * n_gr
    assert per_group == n_fs
    tok_count, top = routes.shape
    width = tokens.shape[1]
    depth = rows * n_fs
    units = depth // n_tp

    cfg = Config()
    cfg.dims = dims
    cfg.inner = inner = 2 if n_fs % 2 == 0 else 1
    cfg.nz = nz = n_fs // inner
    part = tok_count // n_tp
    cfg.R = R = -(-part // 16) * 16
    cfg.CT = CT = min(256, cols, depth)
    cfg.NT = NT = width // CT
    tiles = NT // n_tp
    cfg.DG = DG = 2 if tiles % 2 == 0 and tiles > 1 else 1
    cfg.extra = extra = -(-2 * count // 128) * 128
    chunks = n_gr * depth // CT

    def in_parts(a):
        if R == part:
            return a
        a = jnp.pad(a.reshape(n_tp, part, a.shape[-1]), ((0, 0), (0, R - part), (0, 0)))
        return a.reshape(n_tp * R, a.shape[-1])

    gs, us, dsh = gate_shared, up_shared, down_shared
    cfg.parts = tuple(n_gr if a.shape[0] % (16 * n_gr) == 0 else 1 for a in (gs, us, dsh))
    sds = jax.ShapeDtypeStruct
    outs = (
        sds((n_tp, R, cols), BF),
        sds((n_gr, 1, units, width), BF),
        sds((n_gr, 1, units, width), BF),
        sds((n_gr, 1, depth, cols), BF),
        sds((n_fs * gs.shape[0], gs.shape[1]), BF),
        sds((n_fs * us.shape[0], us.shape[1]), BF),
        sds((n_fs * dsh.shape[0], dsh.shape[1]), BF),
    )
    V, DMA = pltpu.VMEM, pltpu.SemaphoreType.DMA
    q, p, r = max(1, n_tp - 1), max(1, n_gr - 1), max(1, inner - 1)
    M = 2 + DG
    scratch = [
        V((n_fs * R, width + extra), BF),
        V((3, n_gr, depth, width), BF),
        V((n_fs * R, n_gr * depth), BF),
        V(outs[4].shape, BF), V(outs[5].shape, BF), V(outs[6].shape, BF),
        V((n_tp, n_tp * R, gs.shape[1]), BF),
        V((n_tp * R, cols), F32),
        V((NT, r, nz * R, CT), BF), V((NT, r, nz * R, CT), BF),
        V((max(NT, chunks * inner), nz * R, CT), F32),
        V((2, NT, nz * R, CT), BF), V((2, NT, nz * R, CT), BF),
        V((NT, R, CT), BF), V((n_tp, tiles, R, CT), BF),
        V((2, n_fs, rows, cols), F32), V((3, n_fs, rows, cols), BF),
        V(gs.shape, BF), V(us.shape, BF), V(dsh.shape, BF),
        V((n_tp * R, width), BF),
        DMA((3,)),
        DMA((M,)), DMA((M, n_fs)), DMA((M,)), DMA((M, q)), DMA((M, q)),
        DMA((M, n_tp, p)), DMA((M, n_tp, p)),
        DMA((4, 2, nz)), DMA((4, 2, nz)), DMA((4, r, 2 * nz - 1)), DMA((4, r, 2 * nz - 1)),
        DMA((4,)), DMA((4, p)), DMA((4, p)),
        DMA((q,)), DMA((q,)), DMA((NT, r)), DMA((NT, r)), DMA((2, NT)), DMA((2, NT)),
        DMA((NT,)), DMA((n_tp, tiles)), DMA((6, n_gr)),
    ]
    anyw = pl.BlockSpec(memory_space=pl.ANY)
    vmem = pl.BlockSpec(memory_space=pltpu.VMEM)
    held = pl.pallas_call(
        functools.partial(whole, cfg),
        out_shape=tuple(V(o.shape, o.dtype) for o in outs),
        in_specs=[vmem] * 4 + [anyw] * 3 + [vmem] * 3,
        out_specs=(vmem,) * 7,
        scratch_shapes=scratch,
        compiler_params=pltpu.CompilerParams(
            collective_id=1, has_side_effects=True, vmem_limit_bytes=48 << 20),
        cost_estimate=pl.CostEstimate(flops=0, bytes_accessed=200 << 20, transcendentals=0),
    )(in_parts(tokens), in_parts(routes), in_parts(route_weight), norm_gain.reshape(1, width),
      gate_experts[0], up_experts[0], down_experts[0], gs, us, dsh)
    mixed, gate_w, up_w, down_w, gs_w, us_w, ds_w = pl.pallas_call(
        put,
        out_shape=outs,
        in_specs=[vmem] * 7,
        out_specs=(anyw,) * 7,
        scratch_shapes=[DMA((7,))],
        compiler_params=pltpu.CompilerParams(vmem_limit_bytes=1 << 20),
        cost_estimate=pl.CostEstimate(flops=0, bytes_accessed=20 << 20, transcendentals=0),
    )(*held)
    mixed = mixed[:, :part].reshape(tok_count, cols)
    return (mixed, gate_w, up_w, down_w, gs_w, us_w, ds_w)


def put(*refs):
    sems = refs[-1]
    copies = [pltpu.make_async_copy(a, b, sems.at[i]) for i, (a, b) in enumerate(zip(refs[:7], refs[7:14]))]
    for c in copies:
        c.start()
    for c in copies:
        c.wait()


def solution(mesh):
    return jax.shard_map(
        on_device,
        mesh=mesh,
        in_specs=(
            P(("gr", "fs"), None),
            P(("gr", "fs"), None),
            P(("gr", "fs"), None),
            P(),
            P("gr", None, "fs", "tp"),
            P("gr", None, "fs", "tp"),
            P("gr", None, "fs", "tp"),
            P("fs", "tp"),
            P("fs", "tp"),
            P("fs", "tp"),
        ),
        out_specs=(
            P(("gr", "fs"), "tp"),
            P(None, "fs", "tp", None),
            P(None, "fs", "tp", None),
            P(None, "fs", None, "tp"),
            P(None, "tp"),
            P(None, "tp"),
            P(None, "tp"),
        ),
        check_vma=False,
    )
```

time: 223 us -> 174 us (0.78)
  Pallas kernels: 194 us -> 170 us
  local copies, waits for them, and re-layouts: 17.1 us -> 2.91 us
  other arithmetic: 10.4 us -> 0 us
    pallas_call x1 -> x2, Pallas kernels: 194 us -> 170 us  [the longest x1 166 us: on_device(): pl.pallas_call(functools.partial(whole, cfg), out_shape=tuple((V(o.shape,...]
    unnamed x25 -> x2, local copies, waits for them, and re-layouts: 12.9 us -> 2.91 us
    convert_element_type x6 -> x0, other arithmetic: 8.28 us -> none  [the longest x1 3.49 us: on_device(): upper = (up_experts[0] * gain_cols[None, None, :]).astype(BF)]
where the time goes in v2:
time: 174 us
  Pallas kernels  170 us (98%)
  local copies, waits for them, and re-layouts  2.91 us (2%)
    pallas_call x1, Pallas kernels, on_device(): pl.pallas_call(functools.partial(whole, cfg), out_shape=tuple((V(o.shape,...  166 us
    pallas_call x1, Pallas kernels, on_device(): pl.pallas_call(put, out_shape=outs, in_specs=[vmem] * 7, out_specs=(anyw,...  3.81 us

profile of v2, /device:TPU:0, one launch (start us, length us, event | category | flops | bytes accessed | tf_op | source)
XLA Modules:
  0.0 173.5 jit_solution(5262093192825639560)
XLA Ops:
  0.6 1.5 copy.17.route_in
  2.1 1.5 copy.18.weight_in
  3.5 166.2 %shard_map.153 = (bf16[2,96,1024]{2,1,0:T(8,128)(2,1)S(1)}, bf16[2,1,256,2048]{3,2,1,0:T(8,128)(2,1)S(1)}, bf16[2,1,256,2048]{3,2,1,0:T(8,128)(2,1)S(1)}, bf16[2...) custom-call(bf16[192,2048]{1,0:T(8,128)(2,1)} %tok_in.1, ...), custom_call_target="tpu_custom_call" | custom-call | bytes 209715200 | tf_op jit(solution)/shard_map/pallas_call | solution.py:676
  169.7 3.8 %shard_map.154 = (bf16[2,96,1024]{2,1,0:T(8,128)(2,1)}, bf16[2,1,256,2048]{3,2,1,0:T(8,128)(2,1)}, bf16[2,1,256,2048]{3,2,1,0:T(8,128)(2,1)}, bf16[2,1,512,1024]...) custom-call(bf16[2,96,1024]{2,1,0:T(8,128)(2,1)S(1)} %get-tuple-element.21.r, ...), custom_call_target="tpu_custom_call" | custom-call | bytes 20971520 | tf_op jit(solution)/shard_map/pallas_call | solution.py:687

commit v3 on v2

--- a/solution.py
+++ b/solution.py
@@ -15,10 +15,10 @@
 
 def whole(cfg, tok_in, route_in, weight_in, gain_in, gate_in, up_in, down_in, gs_in, us_in, ds_in,
           mixed_o, gate_o, up_o, down_o, gs_o, us_o, ds_o,
-          X, W, H, GS, US, DS, SH, SO, PS, YR, S, ZS, ZR, FS, FR, ST, LB, LG, LU, LD, LN,
+          X, W, H, GS, US, DS, SH, SO, PS, YR, S, ZS, ZR, ZD, FS, FR, RO, ST, LB, LG, LU, LD, LN,
           st_sem, b_send, b_recv, b_own, x_send, x_recv, p_send, p_recv,
           c_zs, c_zr, c_ys, c_yr, c_own, g_send, g_recv,
-          sh_send, sh_recv, y_send, y_recv, z_send, z_recv, f_send, f_recv, o_sem):
+          sh_send, sh_recv, y_send, y_recv, z_send, z_recv, d_send, d_recv, f_send, f_recv, o_sem):
     n_gr, n_fs, n_tp = cfg.dims
     inner, nz, R, NT, CT, DG = cfg.inner, cfg.nz, cfg.R, cfg.NT, cfg.CT, cfg.DG
     gr, fs, tp = lax.axis_index("gr"), lax.axis_index("fs"), lax.axis_index("tp")
@@ -154,23 +154,29 @@
     def token_place(zz, yr):
         return X.at[ds((yr * nz + zz) * R, R), :]
 
-    def shared_item(src, dst, parts):
-        size = src.shape[0] // parts
+    def shared_item(src, dst):
+        size = src.shape[0]
 
         def place(zz, yr):
-            f = zz * inner + (y + yr) % inner
-            if parts == 1:
-                return dst.at[ds(f * size, size), :]
-            return dst.at[ds((f * parts + gr) * size, size), :]
-        return (src if parts == 1 else src.at[ds(gr * size, size), :], place, parts)
-    items = ((token_place(z, 0), token_place, 1),) + tuple(
-        shared_item(s, d, p) for s, d, p in zip((LG, LU, LD), (GS, US, DS), cfg.parts))
+            return dst.at[ds((zz * inner + (y + yr) % inner) * size, size), :]
+        return (src, place)
+    items = ((token_place(z, 0), token_place),) + tuple(
+        shared_item(s, d) for s, d in zip((LG, LU, LD), (GS, US, DS)))
+    carrier = gr == n_gr - 1
+
+    def carried(f):
+        def run(m, *rest):
+            if m:
+                pl.when(carrier)(lambda: f(m, *rest))
+            else:
+                f(m, *rest)
+        return run
 
     def at(way, d):
         return z - d if way == 0 else z + d
 
     def z_copy(m, way, d):
-        own, place, _ = items[m]
+        own, place = items[m]
         dst = place(at(way, d), 0)
         return remote(own if d == 0 else dst, dst, c_zs.at[m, way, d], c_zr.at[m, way, d],
                       (gr, (z + 1 if way == 0 else z - 1) * inner + y, tp))
@@ -179,7 +185,7 @@
         return d + way * (nz - 1) if d else 0
 
     def y_copy(m, q, way, d):
-        own, place, parts = items[m]
+        own, place = items[m]
         zz = at(way, d)
         src = own if d == 0 else place(zz, 0)
         dst = place(zz, inner - q) if m == 0 else place(zz, 0)
@@ -188,7 +194,7 @@
                       (gr, z * inner + (y + q) % inner, tp))
 
     def pass_partner(m, part):
-        if items[m][2] > 1:
+        if m:
             for p in range(1, n_gr):
                 remote(part, part, g_send.at[m, p - 1], g_recv.at[m, p - 1],
                        ((gr + p) % n_gr, fs, tp)).start()
@@ -199,8 +205,9 @@
     def there(d, way):
         return (z - d >= 0) if way == 0 else (z + d < nz)
 
+    @carried
     def gather_start(m):
-        own, place, parts = items[m]
+        own, place = items[m]
         for way in (0, 1):
             pl.when(next_there(way))(lambda way=way: z_copy(m, way, 0).start())
         for q in range(1, inner):
@@ -208,11 +215,13 @@
         if m:
             pltpu.make_async_copy(own, place(z, 0), c_own.at[m]).start()
 
+    @carried
     def gather_own(m):
-        own, place, parts = items[m]
+        own, place = items[m]
         pltpu.make_async_copy(own, place(z, 0), c_own.at[m]).wait()
         pass_partner(m, place(z, 0))
 
+    @carried
     def gather_pass(m, d):
         for way in (0, 1):
             def act(way=way):
@@ -228,6 +237,7 @@
 
     places = [(0, 0)] + [(d, way) for d in range(1, nz) for way in (0, 1)]
 
+    @carried
     def gather_y(m):
         for d, way in places:
             def act(d=d, way=way):
@@ -242,6 +252,7 @@
             else:
                 pl.when(there(d, way))(act)
 
+    @carried
     def gather_sent(m):
         for d, way in places:
             def act(d=d, way=way):
@@ -256,16 +267,14 @@
                 pl.when(there(d, way))(act)
 
     def partner_gathered(m, way):
-        dst = (X, GS, US, DS)[m]
-        if items[m][2] > 1:
-            part = dst.at[pl.ds(0, dst.shape[0] // items[m][2]), :]
-            for p in range(1, n_gr):
-                c = remote(part, part, g_send.at[m, p - 1], g_recv.at[m, p - 1],
-                           ((gr + p) % n_gr, fs, tp))
-                if way:
-                    c.wait_send()
-                else:
-                    c.wait_recv()
+        part = (X, GS, US, DS)[m]
+        for p in range(1, n_gr):
+            c = remote(part, part, g_send.at[m, p - 1], g_recv.at[m, p - 1],
+                       ((gr + p) % n_gr, fs, tp))
+            if way:
+                pl.when(carrier)(c.wait_send)
+            else:
+                pl.when(gr == (n_gr - 1 + p) % n_gr)(c.wait_recv)
 
     per = depth // CT
     chunks = n_gr * per
@@ -301,7 +310,7 @@
     parts = [(1 + k * size, min(n_fs, 1 + (k + 1) * size)) for k in range(stops)]
     gather_start(0)
     keep_own(0)
-    each_other(lambda k: send(0, k), *parts[0])
+    each_other(lambda k: send(0, k), 1, 2)
     convert(1)
     keep_own(1)
     at_row = lax.broadcasted_iota(jnp.int32, (LG.shape[0], width), 0) + fs * LG.shape[0]
@@ -313,8 +322,9 @@
     convert(2)
     if nz > 1:
         gather_pass(0, 1)
-    for part in parts[1:]:
-        each_other(lambda k: send(0, k), *part)
+    each_other(lambda k: send(0, k), 2, n_fs)
+    for m in (1, 2, 3):
+        gather_start(m)
 
     def second(s):
         landed(1, s)
@@ -324,27 +334,25 @@
         if k + 2 < nz - 1 or k + 2 == nz - 1 == 2:
             gather_pass(0, k + 2)
         each_other(lambda s: send(1, s), *part)
+    if nz > 3:
+        gather_pass(0, nz - 1)
     own_block(0).wait()
     share(0, 0)
     for m in range(2, 2 + DG):
         keep_own(m)
+    shared_pass = [(lambda d=d: [gather_pass(m, d) for m in (1, 2, 3)]) for d in range(1, nz)]
     for m in (1, 2, 3):
-        gather_start(m)
+        gather_own(m)
     for k, part in enumerate(parts):
         each_other(second, *part)
         if k == 0:
-            if nz > 3:
-                gather_pass(0, nz - 1)
-            for m in (1, 2, 3):
-                gather_own(m)
             for q in range(1, n_tp):
                 x_landed(0, q)
                 share(0, q)
         if k == max(0, stops - 2):
             gather_y(0)
             lax.fori_loop(0, per, gate_product, 0)
-    shared_pass = [(lambda d=d: [gather_pass(m, d) for m in (1, 2, 3)]) for d in range(1, nz)]
-    for d in range(0, max(0, nz - 3)):
+    for d in range(0, max(1, nz - 3)):
         shared_pass[d]()
     for m in range(3, 2 + DG):
         each_other(lambda k: send(m, k))
@@ -356,8 +364,6 @@
     for q in range(1, n_tp):
         x_landed(1, q)
         share(1, q)
-    for d in range(max(0, nz - 3), max(0, nz - 2)):
-        shared_pass[d]()
 
     def out_wide(m, g):
         return pltpu.make_async_copy(
@@ -381,16 +387,18 @@
         shared_landed(1, q)
     for g in range(n_gr):
         out_wide(1, g).start()
-    for d in range(max(0, nz - 2), nz - 1):
-        shared_pass[d]()
     lax.fori_loop(per, chunks, ahead, 0)
 
     tiles = NT // n_tp
     each_group = tiles // DG
     group = n_tp * each_group
 
+    def offset(i):
+        late = jnp.where(i >= group, 1, 0) if DG > 1 else 0
+        return (i // each_group + late) % n_tp
+
     def owner(i):
-        return (tp + i // each_group % n_tp) % n_tp
+        return (tp + offset(i)) % n_tp
 
     def place_in(i):
         return i // group * each_group + i % each_group
@@ -423,34 +431,44 @@
         m = 2 + a
         if u:
             x_landed(m, u)
-        else:
+        elif a == 0:
             own_block(m).wait()
-        share(m, u)
+        if u or a == 0:
+            share(m, u)
         shared_landed(m, u)
-        base = (a * n_tp + (n_tp - u) % n_tp) * each_group
+        base = (a * n_tp + (n_tp - u - (1 if a else 0)) % n_tp) * each_group
         lax.fori_loop(base, base + each_group, produce, 0)
         tell(base + each_group - 1)
+
+    def make_late(k, u):
+        if k == 0:
+            own_block(3).wait()
+            share(3, 0)
+        make(1, u)
 
     turn = [0] + [n_tp - u for u in range(1, n_tp)]
     for u in turn:
         make(0, u)
-
-    for m in (1, 2, 3):
-        gather_y(m)
-        partner_gathered(m, 0)
-    sg = jnp.dot(LN[...], GS[...], preferred_element_type=F32)
-    su = jnp.dot(LN[...], US[...], preferred_element_type=F32)
-    SH[tp] = (sg / (1.0 + jnp.exp(-sg)) * su).astype(BF)
+    for d in range(max(1, nz - 3), max(1, nz - 2)):
+        shared_pass[d]()
+
     shared_outs = [pltpu.make_async_copy(a, b, o_sem.at[3 + i, 0])
                    for i, (a, b) in enumerate(((GS, gs_o), (US, us_o), (DS, ds_o)))]
-    for c in shared_outs:
-        c.start()
 
     def sh_copy(q):
         return remote(SH.at[tp], SH.at[tp], sh_send.at[q - 1], sh_recv.at[q - 1],
                       (gr, fs, (tp + q) % n_tp))
-    for q in range(1, n_tp):
-        sh_copy(q).start()
+
+    def shared_first():
+        for m in (1, 2, 3):
+            partner_gathered(m, 0)
+        sg = jnp.dot(LN[...], GS[...], preferred_element_type=F32)
+        su = jnp.dot(LN[...], US[...], preferred_element_type=F32)
+        SH[tp] = (sg / (1.0 + jnp.exp(-sg)) * su).astype(BF)
+        for c in shared_outs:
+            c.start()
+        for q in range(1, n_tp):
+            sh_copy(q).start()
 
     def shared_rest():
         for q in range(1, n_tp):
@@ -489,14 +507,34 @@
             ZS[1, i, pl.ds(0, size), :] = S[i, pl.ds(0, size), :].astype(BF)
         z_move(1, i, 0, size, z - 1).start()
 
+    chain = NT - cfg.DT
+
+    def straight(i, to):
+        return remote(ZS.at[0, i, pl.ds(to * R, R), :], ZD.at[i - chain, z],
+                      d_send.at[i - chain, to], d_recv.at[i - chain, z], (gr, to * inner + y, tp))
+
+    def spread(i):
+        ZS[0, i] = S[i].astype(BF)
+        for to in range(nz):
+            pl.when(z != to)(lambda to=to: straight(i, to).start())
+
+    def gather_straight(i):
+        for src in range(nz):
+            @pl.when(z != src)
+            def _(src=src):
+                part = ZD.at[i - chain, src]
+                remote(part, part, d_send.at[i - chain, src], d_recv.at[i - chain, src],
+                       (gr, src * inner + y, tp)).wait_recv()
+                S[i, ds(z * R, R), :] = S[i, ds(z * R, R), :] + ZD[i - chain, src].astype(F32)
+
     def f_copy(i):
         return remote(FS.at[i], FR.at[tp, place_in(i)], f_send.at[i], f_recv.at[tp, place_in(i)],
                       (gr, fs, owner(i)))
 
     def is_mine(i):
-        return i // each_group % n_tp == 0
-
-    def finish(i):
+        return offset(i) == 0
+
+    def end_chain(i):
         if nz > 1:
             last = (nz - 1) * R
 
@@ -509,12 +547,14 @@
             def _():
                 z_move(1, i, 0, R, z + 1).wait_recv()
                 S[i, pl.ds(0, R), :] = S[i, pl.ds(0, R), :] + ZR[1, i, pl.ds(0, R), :].astype(F32)
+
+    def finish(i):
         done = S[i, ds(z * R, R), :]
 
         @pl.when(is_mine(i))
         def _():
             at_cols = ds(place_in(i) * CT, CT)
-            mixed_o[tp, :, at_cols] = (done + SO[ds(tp * R, R), at_cols]).astype(BF)
+            RO[:, at_cols] = done
 
         @pl.when(jnp.logical_not(is_mine(i)))
         def _():
@@ -530,9 +570,10 @@
             def _():
                 each_other(lambda s: landed(3, s), jnp.minimum(n_fs, 1 + j * some),
                            jnp.minimum(n_fs, 1 + (j + 1) * some))
-            for k, u in enumerate(turn):
-                pl.when(j == turns + k)(lambda u=u: make(1, u))
-        pl.when(j == min(2, max(0, nz - 2)))(shared_rest)
+            for k, u in enumerate(turn[1:] + turn[:1]):
+                pl.when(j == turns + k)(lambda k=k, u=u: make_late(k, u))
+        for d in range(max(1, nz - 2), nz - 1):
+            pl.when(j == 1)(lambda d=d: [None, shared_pass[d]()][0])
 
         @pl.when(j < NT)
         def _():
@@ -541,19 +582,38 @@
                 remote(part, part, y_send.at[j, r - 1], y_recv.at[j, r - 1],
                        (gr, z * inner + (y + r) % inner, tp)).wait_recv()
             S[j] = S[j] + sum([YR[j, r - 1].astype(F32) for r in range(1, inner)], 0.0)
+        pl.when((j >= chain) & (j < NT))(lambda: spread(j))
+
+        @pl.when(j == NT - 1)
+        def _():
+            for m in (1, 2, 3):
+                gather_y(m)
+        pl.when(j == NT)(shared_first)
         for h in range(nz - 1):
             i = j - h
 
-            @pl.when((i >= 0) & (i < NT))
+            @pl.when((i >= 0) & (i < chain))
             def _(i=i, h=h):
                 pl.when(z == h)(lambda: upward(i, h))
                 pl.when(z == nz - 1 - h)(lambda: downward(i, h))
         i = j - (nz - 1)
-        pl.when(i >= 0)(lambda: finish(i))
+
+        @pl.when((i >= 0) & (i < chain))
+        def _():
+            end_chain(i)
+            finish(i)
+
+        @pl.when((j > chain) & (j <= NT))
+        def _():
+            gather_straight(j - 1)
+            finish(j - 1)
         return c
-    lax.fori_loop(0, NT + nz - 1, advance, 0)
+    lax.fori_loop(0, max(NT + 1, chain + nz - 1), advance, 0)
     for g in range(n_gr):
         out_tall(g).start()
+
+    shared_rest()
+    mixed_o[tp] = (RO[...] + SO[ds(tp * R, R), :]).astype(BF)
 
     def arrive(i, c):
         for q in range(1, n_tp):
@@ -578,16 +638,24 @@
                 partner(m, gr, q, p).wait_send()
     for m in range(4):
         gather_sent(m)
-        partner_gathered(m, 1)
+        if m:
+            partner_gathered(m, 1)
     for q in range(1, n_tp):
         sh_copy(q).wait_send()
 
     def drain(i, c):
         for r in range(1, inner):
             y_out(i, r).wait_send()
-        for h in range(nz - 1):
-            pl.when(z == h)(lambda h=h: z_move(0, i, (h + 1) * R, (nz - 1 - h) * R, z + 1).wait_send())
-            pl.when(z == nz - 1 - h)(lambda h=h: z_move(1, i, 0, (nz - 1 - h) * R, z - 1).wait_send())
+        @pl.when(i < chain)
+        def _():
+            for h in range(nz - 1):
+                pl.when(z == h)(lambda h=h: z_move(0, i, (h + 1) * R, (nz - 1 - h) * R, z + 1).wait_send())
+                pl.when(z == nz - 1 - h)(lambda h=h: z_move(1, i, 0, (nz - 1 - h) * R, z - 1).wait_send())
+
+        @pl.when(i >= chain)
+        def _():
+            for to in range(nz):
+                pl.when(z != to)(lambda to=to: straight(i, to).wait_send())
         pl.when(jnp.logical_not(is_mine(i)))(lambda: f_copy(i).wait_send())
         return c
     lax.fori_loop(0, NT, drain, 0)
@@ -625,6 +693,7 @@
     cfg.NT = NT = width // CT
     tiles = NT // n_tp
     cfg.DG = DG = 2 if tiles % 2 == 0 and tiles > 1 else 1
+    cfg.DT = 2
     cfg.extra = extra = -(-2 * count // 128) * 128
     chunks = n_gr * depth // CT
 
@@ -635,7 +704,6 @@
         return a.reshape(n_tp * R, a.shape[-1])
 
     gs, us, dsh = gate_shared, up_shared, down_shared
-    cfg.parts = tuple(n_gr if a.shape[0] % (16 * n_gr) == 0 else 1 for a in (gs, us, dsh))
     sds = jax.ShapeDtypeStruct
     outs = (
         sds((n_tp, R, cols), BF),
@@ -659,7 +727,7 @@
         V((NT, r, nz * R, CT), BF), V((NT, r, nz * R, CT), BF),
         V((max(NT, chunks * inner), nz * R, CT), F32),
         V((2, NT, nz * R, CT), BF), V((2, NT, nz * R, CT), BF),
-        V((NT, R, CT), BF), V((n_tp, tiles, R, CT), BF),
+        V((cfg.DT, nz, R, CT), BF), V((NT, R, CT), BF), V((n_tp, tiles, R, CT), BF), V((R, cols), F32),
         V((2, n_fs, rows, cols), F32), V((3, n_fs, rows, cols), BF),
         V(gs.shape, BF), V(us.shape, BF), V(dsh.shape, BF),
         V((n_tp * R, width), BF),
@@ -669,6 +737,7 @@
         DMA((4, 2, nz)), DMA((4, 2, nz)), DMA((4, r, 2 * nz - 1)), DMA((4, r, 2 * nz - 1)),
         DMA((4,)), DMA((4, p)), DMA((4, p)),
         DMA((q,)), DMA((q,)), DMA((NT, r)), DMA((NT, r)), DMA((2, NT)), DMA((2, NT)),
+        DMA((cfg.DT, nz)), DMA((cfg.DT, nz)),
         DMA((NT,)), DMA((n_tp, tiles)), DMA((6, n_gr)),
     ]
     anyw = pl.BlockSpec(memory_space=pl.ANY)

time: 174 us -> 165 us (0.948); the launches traced: 174 us -> 162 us
  Pallas kernels: 170 us -> 158 us
    pallas_call x1, Pallas kernels: 166 us -> 154 us  [on_device(): pl.pallas_call(functools.partial(whole, cfg), out_shape=tuple((V(o.shape,...]
where the time goes in v3:
time: 165 us; the launch traced here: 162 us
  Pallas kernels  158 us (96%)
  local copies, waits for them, and re-layouts  2.91 us (2%)
    pallas_call x1, Pallas kernels, on_device(): pl.pallas_call(functools.partial(whole, cfg), out_shape=tuple((V(o.shape,...  154 us
    pallas_call x1, Pallas kernels, on_device(): pl.pallas_call(put, out_shape=outs, in_specs=[vmem] * 7, out_specs=(anyw,...  3.81 us

profile of v3, /device:TPU:0, one launch (start us, length us, event | category | flops | bytes accessed | tf_op | source)
XLA Modules:
  0.0 161.6 jit_solution(16540439856366368739)
XLA Ops:
  0.6 1.5 copy.17.route_in
  2.1 1.5 copy.18.weight_in
  3.5 154.3 %shard_map.153 = (bf16[2,96,1024]{2,1,0:T(8,128)(2,1)S(1)}, bf16[2,1,256,2048]{3,2,1,0:T(8,128)(2,1)S(1)}, bf16[2,1,256,2048]{3,2,1,0:T(8,128)(2,1)S(1)}, bf16[2...) custom-call(bf16[192,2048]{1,0:T(8,128)(2,1)} %tok_in.1, ...), custom_call_target="tpu_custom_call" | custom-call | bytes 209715200 | tf_op jit(solution)/shard_map/pallas_call | solution.py:745
  157.8 3.8 %shard_map.154 = (bf16[2,96,1024]{2,1,0:T(8,128)(2,1)}, bf16[2,1,256,2048]{3,2,1,0:T(8,128)(2,1)}, bf16[2,1,256,2048]{3,2,1,0:T(8,128)(2,1)}, bf16[2,1,512,1024]...) custom-call(bf16[2,96,1024]{2,1,0:T(8,128)(2,1)S(1)} %get-tuple-element.21.r, ...), custom_call_target="tpu_custom_call" | custom-call | bytes 20971520 | tf_op jit(solution)/shard_map/pallas_call | solution.py:756

commit v4 on v3

--- a/solution.py
+++ b/solution.py
@@ -64,11 +64,13 @@
     lax.fori_loop(0, n_tp * R // 16, normalize, 0)
     mine = ds(tp * R, R)
     X[ds(z * R, R), pl.ds(0, width)] = LN[mine, :]
-    named, shares = route_in[mine, :], weight_in[mine, :]
-    lane = lax.broadcasted_iota(jnp.int32, (R, cfg.extra), 1)
+    own = (lax.broadcasted_iota(jnp.int32, (R, n_tp * R), 0) + tp * R
+           == lax.broadcasted_iota(jnp.int32, (R, n_tp * R), 1))
+    lane = lax.broadcasted_iota(jnp.int32, (R, cfg.extra), 1).astype(F32)
     tail = jnp.zeros((R, cfg.extra), F32)
-    for j in range(named.shape[1]):
-        e, w = named[:, j:j + 1], shares[:, j:j + 1]
+    for j in range(route_in.shape[0]):
+        e = jnp.sum(jnp.where(own, route_in[j:j + 1, :].astype(F32), 0.0), axis=1, keepdims=True)
+        w = jnp.sum(jnp.where(own, weight_in[j:j + 1, :], 0.0), axis=1, keepdims=True)
         high = w.astype(BF).astype(F32)
         tail = tail + jnp.where(lane == e, high, 0.0) + jnp.where(lane == e + count, w - high, 0.0)
     X[ds(z * R, R), pl.ds(width, cfg.extra)] = tail.astype(BF)
@@ -693,7 +695,7 @@
     cfg.NT = NT = width // CT
     tiles = NT // n_tp
     cfg.DG = DG = 2 if tiles % 2 == 0 and tiles > 1 else 1
-    cfg.DT = 2
+    cfg.DT = max(2, NT // 2)
     cfg.extra = extra = -(-2 * count // 128) * 128
     chunks = n_gr * depth // CT
 
@@ -751,7 +753,7 @@
         compiler_params=pltpu.CompilerParams(
             collective_id=1, has_side_effects=True, vmem_limit_bytes=48 << 20),
         cost_estimate=pl.CostEstimate(flops=0, bytes_accessed=200 << 20, transcendentals=0),
-    )(in_parts(tokens), in_parts(routes), in_parts(route_weight), norm_gain.reshape(1, width),
+    )(in_parts(tokens), in_parts(routes).T, in_parts(route_weight).T, norm_gain.reshape(1, width),
       gate_experts[0], up_experts[0], down_experts[0], gs, us, dsh)
     mixed, gate_w, up_w, down_w, gs_w, us_w, ds_w = pl.pallas_call(
         put,

time: 165 us -> 161 us (0.976); the launches traced: 162 us -> 161 us
  local copies, waits for them, and re-layouts: 2.91 us -> 0 us
  Pallas kernels: 158 us -> 160 us
    unnamed x2 -> x0, local copies, waits for them, and re-layouts: 2.91 us -> none
    pallas_call x1, Pallas kernels: 154 us -> 156 us  [on_device(): pl.pallas_call(functools.partial(whole, cfg), out_shape=tuple((V(o.shape,...]
where the time goes in v4:
time: 161 us
  Pallas kernels  160 us (99%)
    pallas_call x1, Pallas kernels, on_device(): pl.pallas_call(functools.partial(whole, cfg), out_shape=tuple((V(o.shape,...  156 us
    pallas_call x1, Pallas kernels, on_device(): pl.pallas_call(put, out_shape=outs, in_specs=[vmem] * 7, out_specs=(anyw,...  3.81 us

profile of v4, /device:TPU:0, one launch (start us, length us, event | category | flops | bytes accessed | tf_op | source)
XLA Modules:
  0.0 160.5 jit_solution(12022791294392929212)
XLA Ops:
  0.6 156.1 %shard_map.153 = (bf16[2,96,1024]{2,1,0:T(8,128)(2,1)S(1)}, bf16[2,1,256,2048]{3,2,1,0:T(8,128)(2,1)S(1)}, bf16[2,1,256,2048]{3,2,1,0:T(8,128)(2,1)S(1)}, bf16[2...) custom-call(bf16[192,2048]{1,0:T(8,128)(2,1)} %tok_in.1, ...), custom_call_target="tpu_custom_call" | custom-call | bytes 209715200 | tf_op jit(solution)/shard_map/pallas_call | solution.py:747
  156.7 3.8 %shard_map.154 = (bf16[2,96,1024]{2,1,0:T(8,128)(2,1)}, bf16[2,1,256,2048]{3,2,1,0:T(8,128)(2,1)}, bf16[2,1,256,2048]{3,2,1,0:T(8,128)(2,1)}, bf16[2,1,512,1024]...) custom-call(bf16[2,96,1024]{2,1,0:T(8,128)(2,1)S(1)} %get-tuple-element.21.r, ...), custom_call_target="tpu_custom_call" | custom-call | bytes 20971520 | tf_op jit(solution)/shard_map/pallas_call | solution.py:758
